TPU v7x, 256 devices: a whole 4x4x8 slice. The times are simulated.
256 devices in a mesh: sp: 32 (over z, x), fs: 4 (over y), tp: 2 (over core).
Axes of the slice: x: 4, y: 4, z: 8, core: 2. Of those that a mesh axis runs over, the one named last changes fastest.
Arguments:
- tokens: bfloat16 [4, 6144, 2048], P('fs', 'sp', 'tp'), may hold values from -24 to 24
- norm_gain: bfloat16 [2048], P('tp'), may hold values from 0.099609375 to 1.8984375
- w_q_down: bfloat16 [2048, 512], P('fs'), may hold values from -0.151 to 0.151
- q_gain: float32 [512], replicated, may hold values from 0.1 to 1.9
- w_q_nope: bfloat16 [512, 2048], P(None, 'tp'), may hold values from -1.21 to 1.21
- w_q_rope: bfloat16 [512, 1024], P(None, 'tp'), may hold values from -0.75 to 0.75
- w_kv_down: bfloat16 [2048, 256], P('fs'), may hold values from -0.151 to 0.151
- kv_gain: float32 [256], replicated, may hold values from 0.1 to 1.9
- w_k_up: bfloat16 [256, 2048], P(None, 'tp'), may hold values from -0.81 to 0.81
- w_v_up: bfloat16 [256, 2048], P(None, 'tp'), may hold values from -0.375 to 0.375
- w_k_rope: bfloat16 [2048, 64], replicated, may hold values from -0.125 to 0.125
- w_pool_in: bfloat16 [2048, 1024], P(None, 'tp'), may hold values from -0.125 to 0.125
- w_pool_mix: bfloat16 [4, 256, 256], replicated, may hold values from -0.375 to 0.375
- w_out_attn: bfloat16 [2048, 2048], P('tp'), may hold values from -0.125 to 0.125
- w_out_pool: bfloat16 [1024, 2048], P('tp'), may hold values from -0.1875 to 0.1875
Outputs:
- mixed: bfloat16 [4, 6144, 2048], P('fs', ('sp', 'tp'))
All inputs are finite; a program needn't handle non-finite values.
Results may differ from a plain program's by a relative error of at most 0.02.
Values may be sent and summed in bfloat16 or wider, within the bound.
A program may use at most 128 MiB of HBM per device.

v0:
```python
import jax
import jax.numpy as jnp
from jax import lax
from jax.sharding import Mesh
from jax.sharding import PartitionSpec as P

NOPE_DIM = 128
ROPE_DIM = 64
VALUE_DIM = 128
GRID_W = 64
POOL_GROUP = 256
SP = ("sp_0", "sp_1")
SP_TP = ("sp_0", "sp_1", "tp")


EPS = 1e-06
THETA = 10000.0
window_sizes = (2, 4, 8, 16)
rim_width = 8
span_limit = 1024


def sent_together(arrays, axis, dim, along):
    both = jnp.concatenate(arrays, axis=along)
    out, at, outs = (lax.all_gather(both, axis, axis=dim, tiled=True), 0, [])
    for a in arrays:
        outs.append(lax.slice_in_dim(out, at, at + a.shape[along], axis=along))
        at += a.shape[along]
    return tuple(outs)


def gathered_by_axis(array, axes, dim):
    out = array
    for number in range(len(axes) - 1, -1, -1):
        out = lax.all_gather(out, axes[number], axis=dim, tiled=True)
    return out


def padded_2(array, sides, width):
    for axis, dim in sides:
        size, length = (lax.axis_size(axis), array.shape[dim])
        up = [(i, (i + 1) % size) for i in range(size - 1)]
        down = [(j, i) for i, j in up]
        last = lax.slice_in_dim(array, length - width, length, axis=dim)
        first = lax.slice_in_dim(array, 0, width, axis=dim)
        before = lax.ppermute(last, axis, up)
        after = lax.ppermute(first, axis, down)
        array = jnp.concatenate([before, array, after], axis=dim)
    return array


def split_up(array, dim, length):
    shape = array.shape
    tiles = array.reshape(*shape[:dim], length, shape[dim] // length, *shape[dim + 1 :])
    return jnp.moveaxis(tiles, dim, 0)


def summed_on_arrival(array, axis, dim):
    tiles = split_up(array, dim, lax.axis_size(axis))
    arrived = lax.all_to_all(tiles, axis, split_axis=0, concat_axis=0, tiled=True)
    return arrived.astype(jnp.float32).sum(axis=0)


def normed(values, gain_vec):
    widened = values.astype(jnp.float32)
    scaled = widened * lax.rsqrt(jnp.mean(widened * widened, axis=-1, keepdims=True) + EPS)
    return (scaled * gain_vec.astype(jnp.float32)).astype(jnp.bfloat16)


def angles(position):
    row_index = (position // GRID_W).astype(jnp.float32)
    column = (position % GRID_W).astype(jnp.float32)
    inverse = THETA ** (-jnp.arange(0, ROPE_DIM // 2, 2).astype(jnp.float32) / (ROPE_DIM // 2))
    return jnp.stack([row_index, column], axis=-1)[:, :, None] * inverse


def rotate(values, angle_table):
    full_shape = values.shape
    split_parts = values.astype(jnp.float32).reshape(full_shape[:-1] + (2, 2, ROPE_DIM // 4))
    front_half = split_parts[..., 0, :]
    back_half = split_parts[..., 1, :]
    cosine = jnp.cos(angle_table)
    sine_part = jnp.sin(angle_table)
    turned = jnp.stack(
        [front_half * cosine - back_half * sine_part, front_half * sine_part + back_half * cosine],
        axis=-2,
    )
    return turned.reshape(full_shape).astype(jnp.bfloat16)


def key_spans(state_now, members, absorb_span):
    row_count = members[0].shape[0]
    span_rows = 1
    for candidate in range(1, min(row_count, span_limit) + 1):
        if row_count % candidate == 0:
            span_rows = candidate
    if span_rows == row_count:
        return absorb_span(state_now, members)
    stacked = tuple(
        (
            member.reshape((row_count // span_rows, span_rows) + member.shape[1:])
            for member in members
        )
    )

    def advance(carry, member_set):
        return (absorb_span(carry, member_set), None)

    final_state, unused = lax.scan(advance, state_now, stacked)
    return final_state


def on_device(
    tokens,
    norm_gain,
    w_q_down,
    q_gain,
    w_q_nope,
    w_q_rope,
    w_kv_down,
    kv_gain,
    w_k_up,
    w_v_up,
    w_k_rope,
    w_pool_in,
    w_pool_mix,
    w_out_attn,
    w_out_pool,
):
    gathered_rows, gathered_gain = (
        lax.all_gather(tokens, "tp", axis=2, tiled=True),
        lax.all_gather(norm_gain, "tp", axis=0, tiled=True),
    )
    token_rows = gathered_rows[0]
    local_rows = token_rows.shape[0]
    q_down, kv_down = sent_together((w_q_down, w_kv_down), "fs", 0, 1)
    heads_dev = w_q_nope.shape[1] // NOPE_DIM
    length = local_rows * lax.axis_size(SP)
    position = lax.axis_index(SP) * local_rows + jnp.arange(local_rows, dtype=jnp.int32)
    angle_table = angles(position)
    hidden = normed(token_rows, gathered_gain)
    q_latent = normed(
        jnp.dot(hidden, q_down, preferred_element_type=jnp.float32).astype(jnp.bfloat16), q_gain
    )
    kv_latent = normed(
        jnp.dot(hidden, kv_down, preferred_element_type=jnp.float32).astype(jnp.bfloat16), kv_gain
    )
    query_nope = jnp.dot(q_latent, w_q_nope, preferred_element_type=jnp.float32).astype(
        jnp.bfloat16
    )
    query_nope = query_nope.reshape(local_rows, heads_dev, NOPE_DIM)
    query_pre = jnp.dot(q_latent, w_q_rope, preferred_element_type=jnp.float32).astype(jnp.bfloat16)
    query_rope = rotate(query_pre.reshape(local_rows, heads_dev, ROPE_DIM), angle_table[:, None])
    key_pre = jnp.dot(hidden, w_k_rope, preferred_element_type=jnp.float32).astype(jnp.bfloat16)
    key_rope = rotate(key_pre, angle_table)
    score_scale = (NOPE_DIM + ROPE_DIM) ** (-0.5)

    def absorb(state_now, key_nope, rope_member, values_all):
        running_max, row_total, weighted = state_now
        key_heads = key_nope.reshape(key_nope.shape[0], heads_dev, NOPE_DIM)
        value_heads = values_all.reshape(values_all.shape[0], heads_dev, VALUE_DIM)
        scores = jnp.einsum(
            "qhd,khd->hqk", query_nope, key_heads, preferred_element_type=jnp.float32
        )
        scores = scores + jnp.einsum(
            "qhr,kr->hqk", query_rope, rope_member, preferred_element_type=jnp.float32
        )
        scores = scores * score_scale
        new_max = jnp.maximum(running_max, jnp.max(scores, axis=-1))
        shrink = jnp.exp(running_max - new_max)
        weights = jnp.exp(scores - new_max[:, :, None])
        row_total = row_total * shrink + jnp.sum(weights, axis=-1)
        weighted = weighted * jnp.transpose(shrink)[:, :, None] + jnp.einsum(
            "hqk,khd->qhd",
            weights.astype(jnp.bfloat16),
            value_heads,
            preferred_element_type=jnp.float32,
        )
        return (new_max, row_total, weighted)

    start_state = (
        jnp.full((heads_dev, local_rows), -1e30, jnp.float32),
        jnp.zeros((heads_dev, local_rows), jnp.float32),
        jnp.zeros((local_rows, heads_dev, VALUE_DIM), jnp.float32),
    )

    def latent_span(state_now, members):
        latent_member, rope_member = members
        key_nope = jnp.dot(latent_member, w_k_up, preferred_element_type=jnp.float32).astype(
            jnp.bfloat16
        )
        values_all = jnp.dot(latent_member, w_v_up, preferred_element_type=jnp.float32).astype(
            jnp.bfloat16
        )
        return absorb(state_now, key_nope, rope_member, values_all)

    final_max, row_total, weighted = key_spans(
        start_state,
        (gathered_by_axis(kv_latent, SP, 0), gathered_by_axis(key_rope, SP, 0)),
        latent_span,
    )
    attended = (weighted / jnp.transpose(row_total)[:, :, None]).astype(jnp.bfloat16)
    attended = attended.reshape(local_rows, heads_dev * VALUE_DIM)
    pool_in = jnp.dot(hidden, w_pool_in, preferred_element_type=jnp.float32).astype(jnp.bfloat16)
    groups_dev = pool_in.shape[1] // POOL_GROUP
    group_id = lax.axis_index("tp") * groups_dev + jnp.arange(groups_dev, dtype=jnp.int32)
    window = jnp.zeros((groups_dev,), jnp.int32)
    for group_index, window_size in enumerate(window_sizes):
        window = window + jnp.where(group_id == group_index, window_size, 0).astype(jnp.int32)
    window = jnp.repeat(window, POOL_GROUP)
    before = window // 2
    window_after = window - before
    padded = padded_2(pool_in, ((SP, 0),), 8)
    padded_wide = padded.astype(jnp.float32)
    window_sum = jnp.zeros(pool_in.shape, jnp.float32)
    for offset in range(-rim_width, rim_width):
        inside = ((offset >= -before) & (offset < window_after)).astype(jnp.float32)
        window_sum = (
            window_sum + padded_wide[rim_width + offset : rim_width + offset + local_rows] * inside
        )
    low_edge = jnp.clip(position[:, None] - before[None, :], 0, length)
    high_edge = jnp.clip(position[:, None] + window_after[None, :], 0, length)
    window_mean = (window_sum / (high_edge - low_edge).astype(jnp.float32)).astype(jnp.bfloat16)
    spread = (window_mean - pool_in).reshape(local_rows, groups_dev, POOL_GROUP)
    mixing = lax.dynamic_slice_in_dim(w_pool_mix, lax.axis_index("tp") * groups_dev, groups_dev, 0)
    pooled = jnp.einsum("tgc,gce->tge", spread, mixing, preferred_element_type=jnp.float32).astype(
        jnp.bfloat16
    )
    pooled = pooled.reshape(local_rows, groups_dev * POOL_GROUP)
    out_share = summed_on_arrival(
        (
            jnp.dot(attended, w_out_attn, preferred_element_type=jnp.float32)
            + jnp.dot(pooled, w_out_pool, preferred_element_type=jnp.float32)
        ).astype(jnp.bfloat16),
        "tp",
        0,
    )
    return out_share.astype(jnp.bfloat16)[None]


def solution(mesh):
    torus = Mesh(
        mesh.devices.reshape(8, 4, mesh.shape["fs"], mesh.shape["tp"]), ("sp_0", "sp_1", "fs", "tp")
    )
    placed = (
        P("fs", SP, "tp"),
        P("tp"),
        P("fs", None),
        P(),
        P(None, "tp"),
        P(None, "tp"),
        P("fs", None),
        P(),
        P(None, "tp"),
        P(None, "tp"),
        P(),
        P(None, "tp"),
        P(),
        P("tp", None),
        P("tp", None),
    )
    return jax.shard_map(
        on_device, mesh=torus, in_specs=placed, out_specs=P("fs", SP_TP, None), check_vma=False
    )
```

profile of v0, /device:TPU:1, one launch (start us, length us, event | category | flops | bytes accessed | tf_op | source)
XLA Modules:
  0.0 248.0 jit_solution(10559850512590616291)
XLA Ops:
  6.5 2.2 pad_maximum_fusion
  8.8 4.7 %all_gather.22 = bf16[2048]{0:T(1024)(128)(2,1)S(1)} all-gather(bf16[1024]{0:T(1024)(128)(2,1)S(1)} %copy-done.11), channel_id=1, replica_groups=mesh['sp_0'=8,'sp_1'=4,'fs'=4,'tp'=2] {'tp'}, dimensions={0}, use_global_device_ids=true | all-gather | bytes 6144 | tf_op jit(solution)/shard_map/all_gather | solution.py:132
  13.5 2.4 all_gather.21
  16.2 38.7 %all-gather.4.cloned.1.call-done = bf16[2048,768]{1,0:T(8,128)(2,1)} async-done(((bf16[512,768]{1,0:T(8,128)(2,1)}), bf16[2048,768]{1,0:T(8,128)(2,1)}) %all-gather.4.cloned.1.call-update) | async-done | bytes 3145744 | tf_op jit(solution)/shard_map/all_gather | solution.py:25
  56.7 11.3 %all_gather.24 = bf16[768,256]{1,0:T(8,128)(2,1)} all-gather(bf16[192,256]{1,0:T(8,128)(2,1)S(1)} %multiply_convert_fusion.1), channel_id=1, replica_groups=mesh['sp_0'=8,'sp_1'=4,'fs'=4,'tp'=2] {'sp_1'}, dimensions={0}, use_global_device_ids=true | all-gather | bytes 491520 | tf_op jit(solution)/shard_map/all_gather | solution.py:35
  68.1 2.3 convolution_convert_fusion.5
  70.4 2.1 collective-permute-start
  74.6 10.5 %all-gather = bf16[4,192,64]{1,2,0:T(8,128)(2,1)S(1)} all-gather(bf16[1,192,64]{1,2,0:T(8,128)(2,1)S(1)} %bitcast.126), channel_id=1, replica_groups=mesh['sp_0'=8,'sp_1'=4,'fs'=4,'tp'=2] {'sp_1'}, dimensions={0}, use_global_device_ids=true | all-gather | bytes 122880 | tf_op jit(solution)/shard_map/all_gather | solution.py:35
  85.7 33.6 %all_gather.27 = bf16[6144,64]{0,1:T(8,128)(2,1)} all-gather(bf16[768,64]{0,1:T(8,128)(2,1)S(1)} %reshape.477), channel_id=1, replica_groups=mesh['sp_0'=8,'sp_1'=4,'fs'=4,'tp'=2] {'sp_0'}, dimensions={0}, use_global_device_ids=true | all-gather | bytes 884736 | tf_op jit(solution)/shard_map/all_gather | solution.py:35
  130.3 93.4 %while.15 = (s32[]{:T(128)}, f32[8,192]{1,0:T(8,128)S(1)}, f32[8,192]{1,0:T(8,128)}, f32[192,8,128]{2,0,1:T(8,128)S(1)}, bf16[6,1024,256]{2,1,0:T(8,128)(2,1)}, ...) while((s32[]{:T(128)}, f32[8,192]{1,0:T(8,128)S(1)}, ...), condition=%wide.region_6.7_spmd.clone, body=%wide.region_3.6_spmd.clone.sunk | while | flops 2094081024 | bytes 63260388 | solution.py:109
  134.2 3.7 %fusion.130 = (f32[8,192]{1,0:T(8,128)S(1)}, f32[8,192,1024]{2,1,0:T(8,128)}) fusion(f32[1024,192,8]{0,1,2:T(8,128)S(1)} %fusion.129, bf16[192,8,128]{2,0,1:T(8,128)(2,1)S(1)} %get-tuple-element.288, bf16[1024,8,128]{0,2,1:T(8,128)(2,1)S(1)} %bitcast.114), kind=kOutput, calls=%fused_computation.160.clone.1 | convolution fusion | flops 407370240 | bytes 15079424 | tf_op jit(solution)/shard_map/while/body/eval_jaxpr/qhd,khd->hqk/dot_general | solution.py:162
  140.0 3.8 %fusion.134 = f32[192,8,128]{2,0,1:T(8,128)S(1)} fusion(bf16[1024,8,128]{0,2,1:T(8,128)(2,1)S(1)} %bitcast.115, f32[8,192,1024]{2,1,0:T(8,128)} %get-tuple-element.256, f32[8,192]{1,0:T(8,128)S(1)} %get-tuple-element.283, f32[192,8,128]{2,0,1:T(8,128)S(1)} %get-tuple-element.273, f32[192,8]{0,1:T(8,128)S(1)} %get-tuple-element.257, pred[]{:T(512)S(6)} %compare.93), kind=kOutput, calls=%fused_computation.10.clone.1 | convolution fusion | flops 406388736 | bytes 9973761 | tf_op jit(solution)/shard_map/while/body/eval_jaxpr/hqk,khd->qhd/dot_general | solution.py:173
  149.7 3.7 %fusion.130 = (f32[8,192]{1,0:T(8,128)S(1)}, f32[8,192,1024]{2,1,0:T(8,128)}) fusion(f32[1024,192,8]{0,1,2:T(8,128)S(1)} %fusion.129, bf16[192,8,128]{2,0,1:T(8,128)(2,1)S(1)} %get-tuple-element.288, bf16[1024,8,128]{0,2,1:T(8,128)(2,1)S(1)} %bitcast.114), kind=kOutput, calls=%fused_computation.160.clone.1 | convolution fusion | flops 407370240 | bytes 15079424 | tf_op jit(solution)/shard_map/while/body/eval_jaxpr/qhd,khd->hqk/dot_general | solution.py:162
  155.6 3.8 %fusion.134 = f32[192,8,128]{2,0,1:T(8,128)S(1)} fusion(bf16[1024,8,128]{0,2,1:T(8,128)(2,1)S(1)} %bitcast.115, f32[8,192,1024]{2,1,0:T(8,128)} %get-tuple-element.256, f32[8,192]{1,0:T(8,128)S(1)} %get-tuple-element.283, f32[192,8,128]{2,0,1:T(8,128)S(1)} %get-tuple-element.273, f32[192,8]{0,1:T(8,128)S(1)} %get-tuple-element.257, pred[]{:T(512)S(6)} %compare.93), kind=kOutput, calls=%fused_computation.10.clone.1 | convolution fusion | flops 406388736 | bytes 9973761 | tf_op jit(solution)/shard_map/while/body/eval_jaxpr/hqk,khd->qhd/dot_general | solution.py:173
  165.3 3.7 %fusion.130 = (f32[8,192]{1,0:T(8,128)S(1)}, f32[8,192,1024]{2,1,0:T(8,128)}) fusion(f32[1024,192,8]{0,1,2:T(8,128)S(1)} %fusion.129, bf16[192,8,128]{2,0,1:T(8,128)(2,1)S(1)} %get-tuple-element.288, bf16[1024,8,128]{0,2,1:T(8,128)(2,1)S(1)} %bitcast.114), kind=kOutput, calls=%fused_computation.160.clone.1 | convolution fusion | flops 407370240 | bytes 15079424 | tf_op jit(solution)/shard_map/while/body/eval_jaxpr/qhd,khd->hqk/dot_general | solution.py:162
  171.1 3.8 %fusion.134 = f32[192,8,128]{2,0,1:T(8,128)S(1)} fusion(bf16[1024,8,128]{0,2,1:T(8,128)(2,1)S(1)} %bitcast.115, f32[8,192,1024]{2,1,0:T(8,128)} %get-tuple-element.256, f32[8,192]{1,0:T(8,128)S(1)} %get-tuple-element.283, f32[192,8,128]{2,0,1:T(8,128)S(1)} %get-tuple-element.273, f32[192,8]{0,1:T(8,128)S(1)} %get-tuple-element.257, pred[]{:T(512)S(6)} %compare.93), kind=kOutput, calls=%fused_computation.10.clone.1 | convolution fusion | flops 406388736 | bytes 9973761 | tf_op jit(solution)/shard_map/while/body/eval_jaxpr/hqk,khd->qhd/dot_general | solution.py:173
  180.9 3.7 %fusion.130 = (f32[8,192]{1,0:T(8,128)S(1)}, f32[8,192,1024]{2,1,0:T(8,128)}) fusion(f32[1024,192,8]{0,1,2:T(8,128)S(1)} %fusion.129, bf16[192,8,128]{2,0,1:T(8,128)(2,1)S(1)} %get-tuple-element.288, bf16[1024,8,128]{0,2,1:T(8,128)(2,1)S(1)} %bitcast.114), kind=kOutput, calls=%fused_computation.160.clone.1 | convolution fusion | flops 407370240 | bytes 15079424 | tf_op jit(solution)/shard_map/while/body/eval_jaxpr/qhd,khd->hqk/dot_general | solution.py:162
  186.7 3.8 %fusion.134 = f32[192,8,128]{2,0,1:T(8,128)S(1)} fusion(bf16[1024,8,128]{0,2,1:T(8,128)(2,1)S(1)} %bitcast.115, f32[8,192,1024]{2,1,0:T(8,128)} %get-tuple-element.256, f32[8,192]{1,0:T(8,128)S(1)} %get-tuple-element.283, f32[192,8,128]{2,0,1:T(8,128)S(1)} %get-tuple-element.273, f32[192,8]{0,1:T(8,128)S(1)} %get-tuple-element.257, pred[]{:T(512)S(6)} %compare.93), kind=kOutput, calls=%fused_computation.10.clone.1 | convolution fusion | flops 406388736 | bytes 9973761 | tf_op jit(solution)/shard_map/while/body/eval_jaxpr/hqk,khd->qhd/dot_general | solution.py:173
  196.4 3.7 %fusion.130 = (f32[8,192]{1,0:T(8,128)S(1)}, f32[8,192,1024]{2,1,0:T(8,128)}) fusion(f32[1024,192,8]{0,1,2:T(8,128)S(1)} %fusion.129, bf16[192,8,128]{2,0,1:T(8,128)(2,1)S(1)} %get-tuple-element.288, bf16[1024,8,128]{0,2,1:T(8,128)(2,1)S(1)} %bitcast.114), kind=kOutput, calls=%fused_computation.160.clone.1 | convolution fusion | flops 407370240 | bytes 15079424 | tf_op jit(solution)/shard_map/while/body/eval_jaxpr/qhd,khd->hqk/dot_general | solution.py:162
  202.2 3.8 %fusion.134 = f32[192,8,128]{2,0,1:T(8,128)S(1)} fusion(bf16[1024,8,128]{0,2,1:T(8,128)(2,1)S(1)} %bitcast.115, f32[8,192,1024]{2,1,0:T(8,128)} %get-tuple-element.256, f32[8,192]{1,0:T(8,128)S(1)} %get-tuple-element.283, f32[192,8,128]{2,0,1:T(8,128)S(1)} %get-tuple-element.273, f32[192,8]{0,1:T(8,128)S(1)} %get-tuple-element.257, pred[]{:T(512)S(6)} %compare.93), kind=kOutput, calls=%fused_computation.10.clone.1 | convolution fusion | flops 406388736 | bytes 9973761 | tf_op jit(solution)/shard_map/while/body/eval_jaxpr/hqk,khd->qhd/dot_general | solution.py:173
  212.0 3.7 %fusion.130 = (f32[8,192]{1,0:T(8,128)S(1)}, f32[8,192,1024]{2,1,0:T(8,128)}) fusion(f32[1024,192,8]{0,1,2:T(8,128)S(1)} %fusion.129, bf16[192,8,128]{2,0,1:T(8,128)(2,1)S(1)} %get-tuple-element.288, bf16[1024,8,128]{0,2,1:T(8,128)(2,1)S(1)} %bitcast.114), kind=kOutput, calls=%fused_computation.160.clone.1 | convolution fusion | flops 407370240 | bytes 15079424 | tf_op jit(solution)/shard_map/while/body/eval_jaxpr/qhd,khd->hqk/dot_general | solution.py:162
  217.8 3.8 %fusion.134 = f32[192,8,128]{2,0,1:T(8,128)S(1)} fusion(bf16[1024,8,128]{0,2,1:T(8,128)(2,1)S(1)} %bitcast.115, f32[8,192,1024]{2,1,0:T(8,128)} %get-tuple-element.256, f32[8,192]{1,0:T(8,128)S(1)} %get-tuple-element.283, f32[192,8,128]{2,0,1:T(8,128)S(1)} %get-tuple-element.273, f32[192,8]{0,1:T(8,128)S(1)} %get-tuple-element.257, pred[]{:T(512)S(6)} %compare.93), kind=kOutput, calls=%fused_computation.10.clone.1 | convolution fusion | flops 406388736 | bytes 9973761 | tf_op jit(solution)/shard_map/while/body/eval_jaxpr/hqk,khd->qhd/dot_general | solution.py:173
  223.7 3.7 %fusion.24 = bf16[192,2048]{1,0:T(8,128)(2,1)S(1)} fusion(f32[192,2048]{1,0:T(8,128)} %fusion.87, bf16[1024,2048]{1,0:T(8,128)(2,1)} %param.30, f32[192,8,128]{2,0,1:T(8,128)S(1)} %get-tuple-element.58, f32[192,8]{0,1:T(8,128)} %bitcast.125), kind=kOutput, calls=%fused_computation.28 | convolution fusion | flops 806486016 | bytes 7346176 | tf_op jit(solution)/shard_map/dot_general | solution.py:232
  227.4 12.8 %all_to_all.5 = bf16[2,96,2048]{2,1,0:T(8,128)(2,1)S(1)} all-to-all(bf16[2,96,2048]{2,1,0:T(8,128)(2,1)S(1)} %bitcast.123), channel_id=1, replica_groups=mesh['sp_0'=8,'sp_1'=4,'fs'=4,'tp'=2] {'tp'}, dimensions={0} | all-to-all | bytes 1572864 | tf_op jit(solution)/shard_map/all_to_all | solution.py:60
  (171 shorter events, 64.7 us)
Async XLA Ops:
  6.5 116.2 %copy-start = (bf16[512,2048]{1,0:T(8,128)(2,1)S(1)}, bf16[512,2048]{1,0:T(8,128)(2,1)}, u32[]{:S(2)}) copy-start(bf16[512,2048]{1,0:T(8,128)(2,1)} %param.31) | copy-start | bytes 6291460
  6.5 2.3 copy-start.11
  6.5 7.0 %copy-start.6 = (bf16[1,192,1024]{2,1,0:T(8,128)(2,1)S(1)}, bf16[1,192,1024]{2,1,0:T(8,128)(2,1)}, u32[]{:S(2)}) copy-start(bf16[1,192,1024]{2,1,0:T(8,128)(2,1)} %param.17) | copy-start | bytes 1179652
  6.5 48.3 %all-gather.4.cloned.1.call-start = ((), (), s32[]{:S(2)}) async-start(), calls=%async_computation.1 | async-start | bytes 3932160 | tf_op jit(solution)/shard_map/all_gather | solution.py:25
  8.8 121.5 %all-gather.6.cloned.1.call-start = ((), (), s32[]{:S(2)}) async-start(), calls=%async_computation.2 | async-start | bytes 3538944 | tf_op jit(solution)/shard_map/all_gather | solution.py:35
  15.9 57.9 %copy-start.1 = (bf16[1,192,2048]{2,1,0:T(8,128)(2,1)}, bf16[1,192,2048]{2,1,0:T(8,128)(2,1)S(1)}, u32[]{:S(2)}) copy-start(bf16[1,192,2048]{2,1,0:T(8,128)(2,1)S(1)} %all_gather.21) | copy-start | bytes 2359300
  15.9 40.7 %copy-start.12 = (f32[256]{0:T(256)S(1)}, f32[256]{0:T(256)}, u32[]{:S(2)}) copy-start(f32[256]{0:T(256)} %param.24) | copy-start | bytes 3076
  68.1 5.8 %copy-start.14 = (bf16[2048,64]{0,1:T(8,128)(2,1)S(1)}, bf16[2048,64]{0,1:T(8,128)(2,1)}, u32[]{:S(2)}) copy-start(bf16[2048,64]{0,1:T(8,128)(2,1)} %param.27) | copy-start | bytes 786436
  70.4 51.0 %collective-permute-start = (bf16[8,512]{1,0:T(8,128)(2,1)S(1)}, bf16[8,512]{1,0:T(8,128)(2,1)S(1)}, u32[]{:S(2)}, u32[]{:S(2)}) collective-permute-start(bf16[8,512]{1,0:T(8,128)(2,1)S(1)} %get-tuple-element.162), channel_id=1, source_target_pairs={{0,8},{8,16},{16,24},{24,32},{32,40},{40,48},{48,56},{56,64},{64,7... | collective-permute-start | bytes 24584 | tf_op jit(solution)/shard_map/ppermute | solution.py:46
  72.5 48.8 %collective-permute-start.1 = (bf16[8,512]{1,0:T(8,128)(2,1)S(1)}, bf16[8,512]{1,0:T(8,128)(2,1)S(1)}, u32[]{:S(2)}, u32[]{:S(2)}) collective-permute-start(bf16[8,512]{1,0:T(8,128)(2,1)S(1)} %get-tuple-element.163), channel_id=1, source_target_pairs={{8,0},{16,8},{24,16},{32,24},{40,32},{48,40},{56,48},{64,56},{72,6... | collective-permute-start | bytes 24584 | tf_op jit(solution)/shard_map/ppermute | solution.py:47
  122.7 2.7 %copy-start.13 = (bf16[2048,768]{1,0:T(8,128)(2,1)S(1)}, bf16[2048,768]{1,0:T(8,128)(2,1)}, u32[]{:S(2)}) copy-start(bf16[2048,768]{1,0:T(8,128)(2,1)} %all-gather.4.cloned.1.call-done) | copy-start | bytes 9437188
  128.2 1.9 copy-start.3
  137.9 5.9 %slice-start = ((s8[6291456]{0:T(1024)(128)(4,1)}), s8[4194304]{0:T(1024)(128)(4,1)S(1)}, s32[]{:S(2)}) async-start(s8[6291456]{0:T(1024)(128)(4,1)} %bitcast.112), calls=%async_computation.3 | async-start | bytes 8388608 | tf_op jit(solution)/shard_map/while
  140.0 3.8 %slice-start.1 = ((s8[6291456]{0:T(1024)(128)(4,1)}), s8[2097152]{0:T(1024)(128)(4,1)S(1)}, s32[]{:S(2)}) async-start(s8[6291456]{0:T(1024)(128)(4,1)} %bitcast.112), calls=%async_computation.4 | async-start | bytes 4194304 | tf_op jit(solution)/shard_map/while
  153.4 5.9 %slice-start = ((s8[6291456]{0:T(1024)(128)(4,1)}), s8[4194304]{0:T(1024)(128)(4,1)S(1)}, s32[]{:S(2)}) async-start(s8[6291456]{0:T(1024)(128)(4,1)} %bitcast.112), calls=%async_computation.3 | async-start | bytes 8388608 | tf_op jit(solution)/shard_map/while
  155.5 3.8 %slice-start.1 = ((s8[6291456]{0:T(1024)(128)(4,1)}), s8[2097152]{0:T(1024)(128)(4,1)S(1)}, s32[]{:S(2)}) async-start(s8[6291456]{0:T(1024)(128)(4,1)} %bitcast.112), calls=%async_computation.4 | async-start | bytes 4194304 | tf_op jit(solution)/shard_map/while
  169.0 5.9 %slice-start = ((s8[6291456]{0:T(1024)(128)(4,1)}), s8[4194304]{0:T(1024)(128)(4,1)S(1)}, s32[]{:S(2)}) async-start(s8[6291456]{0:T(1024)(128)(4,1)} %bitcast.112), calls=%async_computation.3 | async-start | bytes 8388608 | tf_op jit(solution)/shard_map/while
  171.1 3.8 %slice-start.1 = ((s8[6291456]{0:T(1024)(128)(4,1)}), s8[2097152]{0:T(1024)(128)(4,1)S(1)}, s32[]{:S(2)}) async-start(s8[6291456]{0:T(1024)(128)(4,1)} %bitcast.112), calls=%async_computation.4 | async-start | bytes 4194304 | tf_op jit(solution)/shard_map/while
  184.5 5.9 %slice-start = ((s8[6291456]{0:T(1024)(128)(4,1)}), s8[4194304]{0:T(1024)(128)(4,1)S(1)}, s32[]{:S(2)}) async-start(s8[6291456]{0:T(1024)(128)(4,1)} %bitcast.112), calls=%async_computation.3 | async-start | bytes 8388608 | tf_op jit(solution)/shard_map/while
  186.7 3.8 %slice-start.1 = ((s8[6291456]{0:T(1024)(128)(4,1)}), s8[2097152]{0:T(1024)(128)(4,1)S(1)}, s32[]{:S(2)}) async-start(s8[6291456]{0:T(1024)(128)(4,1)} %bitcast.112), calls=%async_computation.4 | async-start | bytes 4194304 | tf_op jit(solution)/shard_map/while
  200.1 5.9 %slice-start = ((s8[6291456]{0:T(1024)(128)(4,1)}), s8[4194304]{0:T(1024)(128)(4,1)S(1)}, s32[]{:S(2)}) async-start(s8[6291456]{0:T(1024)(128)(4,1)} %bitcast.112), calls=%async_computation.3 | async-start | bytes 8388608 | tf_op jit(solution)/shard_map/while
  202.2 3.8 %slice-start.1 = ((s8[6291456]{0:T(1024)(128)(4,1)}), s8[2097152]{0:T(1024)(128)(4,1)S(1)}, s32[]{:S(2)}) async-start(s8[6291456]{0:T(1024)(128)(4,1)} %bitcast.112), calls=%async_computation.4 | async-start | bytes 4194304 | tf_op jit(solution)/shard_map/while
  215.7 5.9 %slice-start = ((s8[6291456]{0:T(1024)(128)(4,1)}), s8[4194304]{0:T(1024)(128)(4,1)S(1)}, s32[]{:S(2)}) async-start(s8[6291456]{0:T(1024)(128)(4,1)} %bitcast.112), calls=%async_computation.3 | async-start | bytes 8388608 | tf_op jit(solution)/shard_map/while
  217.8 3.8 %slice-start.1 = ((s8[6291456]{0:T(1024)(128)(4,1)}), s8[2097152]{0:T(1024)(128)(4,1)S(1)}, s32[]{:S(2)}) async-start(s8[6291456]{0:T(1024)(128)(4,1)} %bitcast.112), calls=%async_computation.4 | async-start | bytes 4194304 | tf_op jit(solution)/shard_map/while
  (17 other events, 18.6 us)
Sparse Core Ops, SparseCore 0:
  9.1 45.6 all-gather.3
  68.2 53.2 all-gather.5
where the time goes:
time: 249 us; the launch traced here: 248 us
  matrix products  93.7 us (38%)
  blocking collectives  75.3 us (30%)
  waiting for transfers between devices  38.8 us (16%)
  between operations  13.7 us (6%)
  other arithmetic  13.5 us (5%)
  local copies, waits for them, and re-layouts  8.98 us (4%)
  starting transfers between devices  3.48 us (1%)
    all_gather x3, blocking collectives, gathered_by_axis(): out = lax.all_gather(out, axes[number], axis=dim, tiled=True)  55.4 us
    all_gather x1, waiting for transfers between devices, sent_together(): out, at, outs = (lax.all_gather(both, axis, axis=dim, tiled=True), 0, [])  38.7 us
    dot_general x6, matrix products, absorb(): jnp.einsum('hqk,khd->qhd', weights.astype(jnp.bfloat16), value_heads, pre...  22.7 us
    dot_general x6, matrix products, absorb(): jnp.einsum('qhd,khd->hqk', query_nope, key_heads, preferred_element_type=...  22 us
    all_to_all x1, blocking collectives, summed_on_arrival(): lax.all_to_all(tiles, axis, split_axis=0, concat_axis=0, tiled=True)  12.8 us
    dot_general x6, matrix products, latent_span(): jnp.dot(latent_member, w_v_up, preferred_element_type=jnp.float32)  12.7 us
    dot_general x6, matrix products, latent_span(): jnp.dot(latent_member, w_k_up, preferred_element_type=jnp.float32)  11.7 us
    dot_general x6, matrix products, absorb(): jnp.einsum('qhr,kr->hqk', query_rope, rope_member, preferred_element_type...  11.6 us
  transfers between devices with their start and end apart: 4, of which 1 were waited for; matrix products, arithmetic and copies ran while one was open for 5% of the time, Pallas kernels for 0%

commit v1 on v0

--- a/solution.py
+++ b/solution.py
@@ -1,6 +1,8 @@
 import jax
 import jax.numpy as jnp
 from jax import lax
+from jax.experimental import pallas as pl
+from jax.experimental.pallas import tpu as pltpu
 from jax.sharding import Mesh
 from jax.sharding import PartitionSpec as P
 
@@ -88,26 +90,91 @@
     return turned.reshape(full_shape).astype(jnp.bfloat16)
 
 
-def key_spans(state_now, members, absorb_span):
-    row_count = members[0].shape[0]
-    span_rows = 1
-    for candidate in range(1, min(row_count, span_limit) + 1):
-        if row_count % candidate == 0:
-            span_rows = candidate
-    if span_rows == row_count:
-        return absorb_span(state_now, members)
-    stacked = tuple(
-        (
-            member.reshape((row_count // span_rows, span_rows) + member.shape[1:])
-            for member in members
+LOG2E = 1.4426950408889634
+KB = 512
+MB = 768
+ROWS = 32
+
+
+def attention_body(q_ref, kv_ref, o_ref, s_scr, p_scr, acc, m_s, l_s):
+    bf, f32 = jnp.bfloat16, jnp.float32
+    chunks = q_ref.shape[0] // MB
+    blocks = kv_ref.shape[0] // KB
+
+    def scores(i, h):
+        k = kv_ref[pl.ds(pl.multiple_of(i * KB, KB), KB), :]
+        s_scr[h] = lax.dot_general(
+            q_ref[h * MB : (h + 1) * MB, :],
+            k,
+            (((1,), (1,)), ((), ())),
+            preferred_element_type=f32,
         )
-    )
-
-    def advance(carry, member_set):
-        return (absorb_span(carry, member_set), None)
-
-    final_state, unused = lax.scan(advance, state_now, stacked)
-    return final_state
+
+    def softmax(h):
+        for r in range(0, MB, ROWS):
+            g = slice(h * MB + r, h * MB + r + ROWS)
+            s = [s_scr[h, r : r + ROWS, j * 128 : (j + 1) * 128] for j in range(KB // 128)]
+            m_old = m_s[g, :]
+            top = s[0]
+            for t in s[1:]:
+                top = jnp.maximum(top, t)
+            m_new = jnp.maximum(m_old, jnp.max(top, axis=1, keepdims=True))
+            alpha = jnp.exp2(m_old - m_new)
+            total = l_s[g, :] * alpha
+            for j, t in enumerate(s):
+                p = jnp.exp2(t - m_new)
+                total = total + p
+                p_scr[h, r : r + ROWS, j * 128 : (j + 1) * 128] = p.astype(bf)
+            m_s[g, :] = m_new
+            l_s[g, :] = total
+            for j in range(2):
+                c = slice(j * 128, (j + 1) * 128)
+                acc[g, c] = acc[g, c] * alpha
+
+    def product(i, h):
+        g = slice(h * MB, (h + 1) * MB)
+        v = kv_ref[pl.ds(pl.multiple_of(i * KB, KB), KB), :256]
+        acc[g, :] = acc[g, :] + jnp.dot(p_scr[h], v, preferred_element_type=f32)
+
+    m_s[...] = jnp.full(m_s.shape, -1e30, f32)
+    l_s[...] = jnp.zeros(l_s.shape, f32)
+    acc[...] = jnp.zeros(acc.shape, f32)
+    p_scr[...] = jnp.zeros(p_scr.shape, bf)
+    scores(0, 0)
+
+    def step(i, c):
+        for h in range(chunks):
+            last = h == chunks - 1
+            scores(jnp.minimum(i + 1, blocks - 1) if last else i, (h + 1) % chunks)
+            softmax(h)
+            product(jnp.maximum(i - 1, 0) if h == 0 else i, (h - 1) % chunks)
+        return c
+
+    lax.fori_loop(0, blocks, step, 0)
+    product(blocks - 1, chunks - 1)
+    for r in range(0, q_ref.shape[0], 128):
+        g = slice(r, r + 128)
+        inv = 1.0 / jnp.sum(l_s[g, :], axis=1, keepdims=True)
+        o_ref[g, :] = (acc[g, :] * inv).astype(bf)
+
+
+def attention(q, kv):
+    rows = q.shape[0]
+    f32 = jnp.float32
+    return pl.pallas_call(
+        attention_body,
+        out_shape=jax.ShapeDtypeStruct((rows, 256), jnp.bfloat16),
+        in_specs=[pl.BlockSpec(memory_space=pltpu.VMEM)] * 2,
+        out_specs=pl.BlockSpec(memory_space=pltpu.VMEM),
+        scratch_shapes=[
+            pltpu.VMEM((rows // MB, MB, KB), f32),
+            pltpu.VMEM((rows // MB, MB, KB), jnp.bfloat16),
+            pltpu.VMEM((rows, 256), f32),
+            pltpu.VMEM((rows, 128), f32),
+            pltpu.VMEM((rows, 128), f32),
+        ],
+        compiler_params=pltpu.CompilerParams(vmem_limit_bytes=48 * 2**20),
+    )(q, kv)
 
 
 def on_device(
@@ -155,51 +222,25 @@
     key_rope = rotate(key_pre, angle_table)
     score_scale = (NOPE_DIM + ROPE_DIM) ** (-0.5)
 
-    def absorb(state_now, key_nope, rope_member, values_all):
-        running_max, row_total, weighted = state_now
-        key_heads = key_nope.reshape(key_nope.shape[0], heads_dev, NOPE_DIM)
-        value_heads = values_all.reshape(values_all.shape[0], heads_dev, VALUE_DIM)
-        scores = jnp.einsum(
-            "qhd,khd->hqk", query_nope, key_heads, preferred_element_type=jnp.float32
-        )
-        scores = scores + jnp.einsum(
-            "qhr,kr->hqk", query_rope, rope_member, preferred_element_type=jnp.float32
-        )
-        scores = scores * score_scale
-        new_max = jnp.maximum(running_max, jnp.max(scores, axis=-1))
-        shrink = jnp.exp(running_max - new_max)
-        weights = jnp.exp(scores - new_max[:, :, None])
-        row_total = row_total * shrink + jnp.sum(weights, axis=-1)
-        weighted = weighted * jnp.transpose(shrink)[:, :, None] + jnp.einsum(
-            "hqk,khd->qhd",
-            weights.astype(jnp.bfloat16),
-            value_heads,
-            preferred_element_type=jnp.float32,
-        )
-        return (new_max, row_total, weighted)
-
-    start_state = (
-        jnp.full((heads_dev, local_rows), -1e30, jnp.float32),
-        jnp.zeros((heads_dev, local_rows), jnp.float32),
-        jnp.zeros((local_rows, heads_dev, VALUE_DIM), jnp.float32),
-    )
-
-    def latent_span(state_now, members):
-        latent_member, rope_member = members
-        key_nope = jnp.dot(latent_member, w_k_up, preferred_element_type=jnp.float32).astype(
-            jnp.bfloat16
-        )
-        values_all = jnp.dot(latent_member, w_v_up, preferred_element_type=jnp.float32).astype(
-            jnp.bfloat16
-        )
-        return absorb(state_now, key_nope, rope_member, values_all)
-
-    final_max, row_total, weighted = key_spans(
-        start_state,
-        (gathered_by_axis(kv_latent, SP, 0), gathered_by_axis(key_rope, SP, 0)),
-        latent_span,
-    )
-    attended = (weighted / jnp.transpose(row_total)[:, :, None]).astype(jnp.bfloat16)
+    q_abs = jnp.einsum(
+        "thd,chd->htc",
+        query_nope,
+        w_k_up.reshape(-1, heads_dev, NOPE_DIM),
+        preferred_element_type=jnp.float32,
+    ) * (score_scale * LOG2E)
+    q_rot = jnp.transpose(query_rope, (1, 0, 2)).astype(jnp.float32) * (score_scale * LOG2E)
+    q_all = jnp.concatenate(
+        [q_abs.astype(jnp.bfloat16), q_rot.astype(jnp.bfloat16), jnp.zeros_like(query_rope).transpose(1, 0, 2)],
+        axis=2,
+    ).reshape(heads_dev * local_rows, 384)
+    kv_dev = jnp.concatenate([kv_latent, key_rope, jnp.zeros_like(key_rope)], axis=1)
+    out_latent = attention(q_all, gathered_by_axis(kv_dev, SP, 0))
+    attended = jnp.einsum(
+        "htc,chd->thd",
+        out_latent.reshape(heads_dev, local_rows, 256),
+        w_v_up.reshape(-1, heads_dev, VALUE_DIM),
+        preferred_element_type=jnp.float32,
+    ).astype(jnp.bfloat16)
     attended = attended.reshape(local_rows, heads_dev * VALUE_DIM)
     pool_in = jnp.dot(hidden, w_pool_in, preferred_element_type=jnp.float32).astype(jnp.bfloat16)
     groups_dev = pool_in.shape[1] // POOL_GROUP

time: 249 us -> 170 us (0.68)
  matrix products: 93.7 us -> 11.8 us
  blocking collectives: 75.3 us -> 24.1 us
  waiting for transfers between devices: 38.8 us -> 84.3 us
  Pallas kernels: 0 us -> 23.2 us
  other arithmetic: 13.5 us -> 5.35 us
  local copies, waits for them, and re-layouts: 8.98 us -> 3.62 us
    dot_general x30 -> x2, matrix products: 80.7 us -> 0.72 us  [the longest x1 0.36 us: on_device(): jnp.einsum('thd,chd->htc', query_nope, w_k_up.reshape(-1, heads_dev, NOPE...]
    all_gather x1, waiting for transfers between devices: 0.02 us -> 44.7 us  [gathered_by_axis(): out = lax.all_gather(out, axes[number], axis=dim, tiled=True)]
    all_gather x3 -> x1, blocking collectives: 55.4 us -> 12.2 us  [gathered_by_axis(): out = lax.all_gather(out, axes[number], axis=dim, tiled=True)]
    pallas_call x0 -> x1, Pallas kernels: none -> 23.2 us  [attention(): pl.pallas_call(attention_body, out_shape=jax.ShapeDtypeStruct((rows, 256)...]
    reduce_sum x6 -> x0, other arithmetic: 8.37 us -> none  [absorb(): row_total = row_total * shrink + jnp.sum(weights, axis=-1)]
    all_to_all x1, blocking collectives: 12.8 us -> 4.83 us  [summed_on_arrival(): lax.all_to_all(tiles, axis, split_axis=0, concat_axis=0, tiled=True)]
    while x54 -> x0, local copies, waits for them, and re-layouts: 3.58 us -> none
    dot_general x1, matrix products: 3.73 us -> 0.99 us  [on_device(): jnp.dot(attended, w_out_attn, preferred_element_type=jnp.float32)]
  transfers between devices with their start and end apart: 4 -> 4, of which waited for: 1 -> 3; matrix products, arithmetic and copies ran while one was open for 5% -> 7% of each run, Pallas kernels for 0% -> 0%
where the time goes in v1:
time: 170 us; the launch traced here: 169 us
  waiting for transfers between devices  84.3 us (50%)
  blocking collectives  24.1 us (14%)
  Pallas kernels  23.2 us (14%)
  between operations  13.8 us (8%)
  matrix products  11.8 us (7%)
  other arithmetic  5.35 us (3%)
  local copies, waits for them, and re-layouts  3.62 us (2%)
  starting transfers between devices  2.99 us (2%)
    all_gather x1, waiting for transfers between devices, gathered_by_axis(): out = lax.all_gather(out, axes[number], axis=dim, tiled=True)  44.7 us
    all_gather x1, waiting for transfers between devices, sent_together(): out, at, outs = (lax.all_gather(both, axis, axis=dim, tiled=True), 0, [])  36.8 us
    pallas_call x1, Pallas kernels, attention(): pl.pallas_call(attention_body, out_shape=jax.ShapeDtypeStruct((rows, 256)...  23.2 us
    all_gather x1, blocking collectives, gathered_by_axis(): out = lax.all_gather(out, axes[number], axis=dim, tiled=True)  12.2 us
    all_to_all x1, blocking collectives, summed_on_arrival(): lax.all_to_all(tiles, axis, split_axis=0, concat_axis=0, tiled=True)  4.83 us
    all_gather x1, blocking collectives, on_device(): lax.all_gather(norm_gain, 'tp', axis=0, tiled=True)  4.7 us
  transfers between devices with their start and end apart: 4, of which 3 were waited for; matrix products, arithmetic and copies ran while one was open for 7% of the time, Pallas kernels for 0%

profile of v1, /device:TPU:1, one launch (start us, length us, event | category | flops | bytes accessed | tf_op | source)
XLA Modules:
  0.0 169.2 jit_solution(13449725713692445551)
XLA Ops:
  6.5 2.2 %pad_maximum_fusion = bf16[512,768]{1,0:T(8,128)(2,1)} fusion(bf16[512,256]{1,0:T(8,128)(2,1)} %param.21, bf16[512,512]{1,0:T(8,128)(2,1)} %param.17), kind=kLoop, calls=%fused_computation.26 | loop fusion | flops 1572864 | bytes 1572864 | tf_op jit(solution)/shard_map/concatenate | solution.py:26
  8.9 4.7 %all_gather.16 = bf16[2048]{0:T(1024)(128)(2,1)S(1)} all-gather(bf16[1024]{0:T(1024)(128)(2,1)S(1)} %copy-done.10), channel_id=1, replica_groups=mesh['sp_0'=8,'sp_1'=4,'fs'=4,'tp'=2] {'tp'}, dimensions={0}, use_global_device_ids=true | all-gather | bytes 6144 | tf_op jit(solution)/shard_map/all_gather | solution.py:199
  13.6 2.4 %all_gather.15 = bf16[1,192,2048]{2,1,0:T(8,128)(2,1)S(1)} all-gather(bf16[1,192,1024]{2,1,0:T(8,128)(2,1)S(1)} %copy-done.7), channel_id=1, replica_groups=mesh['sp_0'=8,'sp_1'=4,'fs'=4,'tp'=2] {'tp'}, dimensions={2}, use_global_device_ids=true | all-gather | bytes 1179648 | tf_op jit(solution)/shard_map/all_gather | solution.py:198
  16.2 1.4 convolution_convert_fusion.6
  18.1 36.8 %all-gather.3.cloned.1.call-done = bf16[2048,768]{1,0:T(8,128)(2,1)} async-done(((bf16[512,768]{1,0:T(8,128)(2,1)}), bf16[2048,768]{1,0:T(8,128)(2,1)}) %all-gather.3.cloned.1.call-update) | async-done | bytes 3145744 | tf_op jit(solution)/shard_map/all_gather | solution.py:27
  54.9 1.7 %multiply_reduce_fusion.1 = (f32[192]{0:T(256)S(1)}, f32[192,256]{1,0:T(8,128)S(1)}) fusion(bf16[2048,768]{1,0:T(8,128)(2,1)} %all-gather.3.cloned.1.call-done, bf16[1,192,2048]{2,1,0:T(8,128)(2,1)S(1)} %all_gather.15, f32[2048]{0:T(1024)S(1)} %convert_element_type.242, f32[192]{0:T(256)S(1)} %add_rsqrt_fusion.2), kind=kOutput, calls=%fused_computation.78 | convolution fusion | flops 203095872 | bytes 2041344 | tf_op jit(solution)/shard_map/dot_general | solution.py:213
  56.8 12.2 %all_gather.18 = bf16[768,384]{1,0:T(8,128)(2,1)} all-gather(bf16[192,384]{1,0:T(8,128)(2,1)S(1)} %maximum_maximum_fusion.1), channel_id=1, replica_groups=mesh['sp_0'=8,'sp_1'=4,'fs'=4,'tp'=2] {'sp_1'}, dimensions={0}, use_global_device_ids=true | all-gather | bytes 737280 | tf_op jit(solution)/shard_map/all_gather | solution.py:37
  69.0 2.2 %convolution_convert_fusion.4 = bf16[192,512]{1,0:T(8,128)(2,1)S(1)} fusion(bf16[2048,512]{1,0:T(8,128)(2,1)} %param.26, bf16[1,192,2048]{2,1,0:T(8,128)(2,1)S(1)} %all_gather.15, f32[2048]{0:T(1024)S(1)} %convert_element_type.242, f32[192]{0:T(256)S(1)} %add_rsqrt_fusion.2), kind=kOutput, calls=%fused_computation.20 | convolution fusion | flops 404324352 | bytes 3089152 | tf_op jit(solution)/shard_map/dot_general | solution.py:245
  71.3 1.7 collective-permute-start
  72.9 1.3 collective-permute-start.1
  74.6 2.7 %collective-permute-done.1 = bf16[8,512]{1,0:T(8,128)(2,1)S(1)} collective-permute-done((bf16[8,512]{1,0:T(8,128)(2,1)S(1)}, bf16[8,512]{1,0:T(8,128)(2,1)S(1)}, u32[]{:S(2)}, u32[]{:S(2)}) %collective-permute-start.1) | collective-permute-done | bytes 8224 | tf_op jit(solution)/shard_map/ppermute | solution.py:49
  77.4 0.8 fusion.46
  78.7 1.8 %fusion.68 = f32[192,2048]{1,0:T(8,128)} fusion(bf16[192,512]{1,0:T(8,128)(2,1)S(1)} %bitcast.73, bf16[512,2048]{1,0:T(8,128)(2,1)S(1)} %copy-done), kind=kOutput, calls=%fused_computation.141 | convolution fusion | flops 402653184 | bytes 3866624 | tf_op jit(solution)/shard_map/dot_general | solution.py:274
  80.5 0.6 copy-done.12
  81.1 0.7 multiply_reduce_fusion
  82.9 0.9 copy.36
  83.8 1.7 %fusion.6 = bf16[24,8,8,128]{3,2,1,0:T(8,128)(2,1)S(1)} fusion(bf16[512,1024]{1,0:T(8,128)(2,1)} %param.19, f32[192,512]{1,0:T(8,128)S(1)} %get-tuple-element.32, f32[512]{0:T(512)S(1)} %copy-done.9, f32[192]{0:T(256)S(1)} %add_rsqrt_fusion.1), kind=kOutput, calls=%fused_computation.12 | convolution fusion | flops 201818112 | bytes 1837824 | tf_op jit(solution)/shard_map/dot_general | solution.py:215
  85.5 0.4 multiply_convert_fusion
  86.1 44.7 %all-gather.5.cloned.1.call-done.kv_ref = bf16[6144,384]{1,0:T(8,128)(2,1)} async-done(((bf16[768,384]{1,0:T(8,128)(2,1)}), bf16[6144,384]{1,0:T(8,128)(2,1)}) %all-gather.5.cloned.1.call-update) | async-done | bytes 4718608 | tf_op jit(solution)/shard_map/all_gather | solution.py:37
  130.9 23.2 %shard_map.145 = bf16[1536,256]{1,0:T(8,128)(2,1)S(1)} custom-call(bf16[1536,384]{1,0:T(8,128)(2,1)S(1)} %bitcast.66, bf16[6144,384]{1,0:T(8,128)(2,1)} %all-gather.5.cloned.1.call-done.kv_ref), custom_call_target="tpu_custom_call" | custom-call | tf_op jit(solution)/shard_map/pallas_call | solution.py:164
  154.5 1.0 copy-done.1
  155.5 1.0 fusion
  156.5 4.8 %all_to_all.5 = bf16[2,96,2048]{2,1,0:T(8,128)(2,1)S(1)} all-to-all(bf16[2,96,2048]{2,1,0:T(8,128)(2,1)S(1)} %bitcast.68), channel_id=1, replica_groups=mesh['sp_0'=8,'sp_1'=4,'fs'=4,'tp'=2] {'tp'}, dimensions={0} | all-to-all | bytes 1572864 | tf_op jit(solution)/shard_map/all_to_all | solution.py:62
  161.3 1.0 reduce_sum.42
  (62 shorter events, 3.3 us)
Async XLA Ops:
  6.5 72.1 %copy-start = (bf16[512,2048]{1,0:T(8,128)(2,1)S(1)}, bf16[512,2048]{1,0:T(8,128)(2,1)}, u32[]{:S(2)}) copy-start(bf16[512,2048]{1,0:T(8,128)(2,1)} %param.29) | copy-start | bytes 6291460
  6.5 2.3 %copy-start.10 = (bf16[1024]{0:T(1024)(128)(2,1)S(1)}, bf16[1024]{0:T(1024)(128)(2,1)}, u32[]{:S(2)}) copy-start(bf16[1024]{0:T(1024)(128)(2,1)} %param.16) | copy-start | bytes 6148
  6.5 7.0 %copy-start.7 = (bf16[1,192,1024]{2,1,0:T(8,128)(2,1)S(1)}, bf16[1,192,1024]{2,1,0:T(8,128)(2,1)}, u32[]{:S(2)}) copy-start(bf16[1,192,1024]{2,1,0:T(8,128)(2,1)} %param.15) | copy-start | bytes 1179652
  6.5 48.3 %all-gather.3.cloned.1.call-start = ((), (), s32[]{:S(2)}) async-start(), calls=%async_computation.1 | async-start | bytes 3932160 | tf_op jit(solution)/shard_map/all_gather | solution.py:27
  8.8 122.1 %all-gather.5.cloned.1.call-start = ((), (), s32[]{:S(2)}) async-start(), calls=%async_computation.2 | async-start | bytes 5308416 | tf_op jit(solution)/shard_map/all_gather | solution.py:37
  18.0 38.6 %copy-start.11 = (f32[256]{0:T(256)S(1)}, f32[256]{0:T(256)}, u32[]{:S(2)}) copy-start(f32[256]{0:T(256)} %param.22) | copy-start | bytes 3076
  71.3 3.3 %collective-permute-start = (bf16[8,512]{1,0:T(8,128)(2,1)S(1)}, bf16[8,512]{1,0:T(8,128)(2,1)S(1)}, u32[]{:S(2)}, u32[]{:S(2)}) collective-permute-start(bf16[8,512]{1,0:T(8,128)(2,1)S(1)} %get-tuple-element.10), channel_id=1, source_target_pairs={{0,8},{8,16},{16,24},{24,32},{32,40},{40,48},{48,56},{56,64},{64,7... | collective-permute-start | bytes 24584 | tf_op jit(solution)/shard_map/ppermute | solution.py:48
  72.9 4.4 %collective-permute-start.1 = (bf16[8,512]{1,0:T(8,128)(2,1)S(1)}, bf16[8,512]{1,0:T(8,128)(2,1)S(1)}, u32[]{:S(2)}, u32[]{:S(2)}) collective-permute-start(bf16[8,512]{1,0:T(8,128)(2,1)S(1)} %get-tuple-element.11), channel_id=1, source_target_pairs={{8,0},{16,8},{24,16},{32,24},{40,32},{48,40},{56,48},{64,56},{72,6... | collective-permute-start | bytes 24584 | tf_op jit(solution)/shard_map/ppermute | solution.py:49
  77.4 1.0 copy-start.8
  78.7 2.5 %copy-start.12 = (bf16[2048,768]{1,0:T(8,128)(2,1)S(1)}, bf16[2048,768]{1,0:T(8,128)(2,1)}, u32[]{:S(2)}) copy-start(bf16[2048,768]{1,0:T(8,128)(2,1)} %all-gather.3.cloned.1.call-done) | copy-start | bytes 9437188
  81.1 1.0 copy-start.4
  81.1 1.0 copy-start.9
  82.8 2.7 %copy-start.5 = (bf16[256,1024]{1,0:T(8,128)(2,1)S(1)}, bf16[256,1024]{1,0:T(8,128)(2,1)}, u32[]{:S(2)}) copy-start(bf16[256,1024]{1,0:T(8,128)(2,1)} %param.23) | copy-start | bytes 1572868
  83.8 2.1 %copy-start.3 = (bf16[192,8,64]{2,0,1:T(8,128)(2,1)S(1)}, bf16[192,8,64]{2,0,1:T(8,128)(2,1)}, u32[]{:S(2)}) copy-start(bf16[192,8,64]{2,0,1:T(8,128)(2,1)} %copy.36) | copy-start | bytes 589828
  130.9 23.2 %copy-start.6 = (bf16[256,1024]{1,0:T(8,128)(2,1)S(1)}, bf16[256,1024]{1,0:T(8,128)(2,1)}, u32[]{:S(2)}) copy-start(bf16[256,1024]{1,0:T(8,128)(2,1)} %param.24) | copy-start | bytes 1572868
  130.9 23.6 %copy-start.2 = (bf16[1024,2048]{1,0:T(8,128)(2,1)S(1)}, bf16[1024,2048]{1,0:T(8,128)(2,1)}, u32[]{:S(2)}) copy-start(bf16[1024,2048]{1,0:T(8,128)(2,1)} %param.28) | copy-start | bytes 12582916
  154.1 1.4 copy-start.1
Sparse Core Ops, SparseCore 0:
  9.1 45.6 all-gather.2
  69.1 61.7 all-gather.4

commit v2 on v1

v2 whole, which is shorter than its diff:
```python
import functools

import jax
import jax.numpy as jnp
import numpy as np
from jax import lax
from jax.experimental import pallas as pl
from jax.experimental.pallas import tpu as pltpu
from jax.sharding import Mesh
from jax.sharding import PartitionSpec as P

NOPE_DIM = 128
ROPE_DIM = 64
VALUE_DIM = 128
GRID_W = 64
POOL_GROUP = 256
SP = ("sp_0", "sp_1")
SP_TP = ("sp_0", "sp_1", "tp")
EPS = 1e-06
THETA = 10000.0
LOG2E = 1.4426950408889634
MESH = pl.DeviceIdType.MESH

NZ, NX, NY = 8, 4, 4
TOK = 192
HALF = 96
D = 2048
HEADS = 8
QR, KR = 512, 256
WIDE = 384
UNIT = 384
ROWS = HEADS * TOK
MB = 768
SUB = 32
SEQ = NZ * NX * TOK
SCALE = (NOPE_DIM + ROPE_DIM) ** (-0.5) * LOG2E
f32, bf16 = jnp.float32, jnp.bfloat16


def rope_tables():
    inverse = (THETA ** (-np.arange(0, ROPE_DIM // 2, 2) / (ROPE_DIM // 2))).astype(np.float32)
    lane = np.arange(128)
    freq = inverse[lane % 16]
    by_row = (lane // 32) % 2 == 0
    sign = np.where((lane // 16) % 2 == 0, -1.0, 1.0)

    def table(count, keep):
        angle = (np.arange(count, dtype=np.float32)[:, None] * freq).astype(np.float64)
        cos = np.where(keep, np.cos(angle), 0.0)
        sin = np.where(keep, np.sin(angle) * sign, 0.0)
        return np.stack([cos, sin]).astype(np.float32)

    return table(SEQ // GRID_W, by_row), table(GRID_W, ~by_row)


def turned(values, cos, sin):
    lane = lax.broadcasted_iota(jnp.int32, values.shape, 1)
    ahead = pltpu.roll(values, 112, 1)
    behind = pltpu.roll(values, 16, 1)
    partner = jnp.where((lane // 16) % 2 == 0, ahead, behind)
    return values * cos + partner * sin


def scaled_rows(values, gain, width):
    mean = jnp.sum(values * values, axis=1, keepdims=True) * (1.0 / width)
    return values * lax.rsqrt(mean + EPS) * gain


def layer_body(
    tokens,
    norm_gain,
    w_q_down,
    q_gain,
    w_q_nope,
    w_q_rope,
    w_kv_down,
    kv_gain,
    w_k_up,
    w_v_up,
    w_k_rope,
    w_pool_in,
    w_pool_mix,
    w_out_attn,
    w_out_pool,
    row_table,
    col_table,
    out,
    tok,
    gains,
    hidden,
    wkv,
    wq,
    wkr,
    wpi,
    wqn,
    wqr,
    wku,
    wvu,
    mix,
    woa,
    wop,
    cos_s,
    sin_s,
    kv,
    q_all,
    q_lat,
    q_nope,
    pool_in,
    halo,
    pooled,
    out_sum,
    att,
    send_buf,
    recv_buf,
    s_scr,
    p_scr,
    acc,
    m_s,
    l_s,
    loc,
    tok_ss,
    tok_rs,
    w_ss,
    w_rs,
    ws_ss,
    ws_rs,
    p1_ss,
    p1_rs,
    ring_ss,
    ring_rs,
    sib_ss,
    sib_rs,
    halo_ss,
    halo_rs,
    out_ss,
    out_rs,
):
    z, x = lax.axis_index("sp_0"), lax.axis_index("sp_1")
    y, c = lax.axis_index("fs"), lax.axis_index("tp")
    sp = z * NX + x
    other = {"tp": 1 - c}
    y_up, y_down = {"fs": lax.rem(y + 1, NY)}, {"fs": lax.rem(y + NY - 1, NY)}
    z_up, z_down = {"sp_0": lax.rem(z + 1, NZ)}, {"sp_0": lax.rem(z + NZ - 1, NZ)}
    x_up, x_down = {"sp_1": lax.rem(x + 1, NX)}, {"sp_1": lax.rem(x + NX - 1, NX)}
    sp_next, sp_prev = lax.rem(sp + 1, NZ * NX), lax.rem(sp + NZ * NX - 1, NZ * NX)
    next_dev = {"sp_0": sp_next // NX, "sp_1": sp_next % NX}
    prev_dev = {"sp_0": sp_prev // NX, "sp_1": sp_prev % NX}

    def remote(src, dst, ssem, rsem, dev):
        return pltpu.make_async_remote_copy(
            src_ref=src, dst_ref=dst, send_sem=ssem, recv_sem=rsem, device_id=dev, device_id_type=MESH
        )

    def local(i, src, dst):
        return pltpu.make_async_copy(src, dst, loc.at[i])

    loads = [
        local(0, tokens, tok.at[c]),
        local(1, norm_gain, gains.at[c]),
        local(2, w_kv_down, wkv.at[pl.ds(y * 512, 512)]),
        local(3, w_k_rope, wkr),
        local(4, w_pool_in, wpi),
        local(5, w_q_down, wq.at[pl.ds(y * 512, 512)]),
        local(6, w_pool_mix.at[pl.ds(2 * c, 2)], mix),
        local(7, w_out_pool, wop),
        local(8, w_q_nope, wqn),
        local(9, w_q_rope, wqr),
        local(10, w_k_up, wku),
        local(11, w_v_up, wvu),
        local(12, w_out_attn, woa),
    ]
    for copy in loads:
        copy.start()

    barrier = pltpu.get_barrier_semaphore()
    partners = [other, y_up, y_down, next_dev, prev_dev]
    partners += [{"sp_0": lax.rem(z + i, NZ)} for i in range(1, NZ)]
    partners += [{"sp_1": lax.rem(x + i, NX)} for i in range(1, NX)]
    for dev in partners:
        pl.semaphore_signal(barrier, inc=1, device_id=dev, device_id_type=MESH)
    pl.semaphore_wait(barrier, len(partners))

    tok_copy = remote(tokens, tok.at[c], tok_ss.at[0], tok_rs.at[0], other)
    gain_copy = remote(norm_gain, gains.at[c], tok_ss.at[1], tok_rs.at[1], other)
    tok_copy.start()
    gain_copy.start()

    def shard_rows(of, part, count):
        return pl.ds(of * 512 + c * 256 + part * 128, count)

    y1, y2, y3 = lax.rem(y + 3, NY), lax.rem(y + 1, NY), lax.rem(y + 2, NY)

    def weight_copies(w, hbm, buf):
        own_a, own_b = hbm.at[pl.ds(c * 256, 128)], hbm.at[pl.ds(c * 256 + 128, 128)]
        dst_a, dst_b = buf.at[shard_rows(y, 0, 128)], buf.at[shard_rows(y, 1, 128)]
        low, high = buf.at[shard_rows(y1, 0, 128)], buf.at[shard_rows(y2, 1, 128)]
        ss, rs = w_ss.at[w], w_rs.at[w]
        return dict(
            up1=remote(own_a, dst_a, ss.at[0], rs.at[0], y_up),
            up2=remote(own_b, dst_b, ss.at[1], rs.at[1], y_up),
            dn1=remote(own_b, dst_b, ss.at[2], rs.at[2], y_down),
            dn2=remote(own_a, dst_a, ss.at[3], rs.at[3], y_down),
            upf=remote(low, low, ss.at[4], rs.at[4], y_up),
            dnf=remote(high, high, ss.at[5], rs.at[5], y_down),
        )

    def weight_arrivals(w, hbm, buf):
        ss, rs = w_ss.at[w], w_rs.at[w]

        def got(i, of, part):
            view = buf.at[shard_rows(of, part, 128)]
            return remote(view, view, ss.at[i], rs.at[i], y_up)

        return dict(
            up1=got(0, y1, 0), up2=got(1, y1, 1), dn1=got(2, y2, 1), dn2=got(3, y2, 0), upf=got(4, y3, 0), dnf=got(5, y3, 1)
        )

    def weight_sibling(w, buf):
        ss, rs = ws_ss.at[w], ws_rs.at[w]
        sends, gots = [], []
        for i, of in enumerate((y1, y2, y3)):
            mine = buf.at[pl.ds(of * 512 + c * 256, 256)]
            theirs = buf.at[pl.ds(of * 512 + (1 - c) * 256, 256)]
            sends.append(remote(mine, mine, ss.at[i], rs.at[i], other))
            gots.append(remote(theirs, theirs, ss.at[i], rs.at[i], other))
        return sends, gots

    kvs, kva = weight_copies(0, w_kv_down, wkv), weight_arrivals(0, w_kv_down, wkv)
    qs, qa = weight_copies(1, w_q_down, wq), weight_arrivals(1, w_q_down, wq)
    kv_sib, kv_sib_got = weight_sibling(0, wkv)
    q_sib, q_sib_got = weight_sibling(1, wq)
    for name in ("up1", "dn1", "up2", "dn2"):
        kvs[name].start()
    for name in ("up1", "dn1"):
        qs[name].start()

    for k in range(TOK // GRID_W):
        rows = slice(k * GRID_W, (k + 1) * GRID_W)
        at = 3 * sp + k
        cos_s[rows, :] = row_table[0, pl.ds(at, 1), :] + col_table[0]
        sin_s[rows, :] = row_table[1, pl.ds(at, 1), :] + col_table[1]

    loads[0].wait()
    loads[1].wait()
    remote(tok.at[1 - c], tok.at[1 - c], tok_ss.at[0], tok_rs.at[0], other).wait_recv()
    remote(gains.at[1 - c], gains.at[1 - c], tok_ss.at[1], tok_rs.at[1], other).wait_recv()
    g0, g1 = gains[0].astype(f32), gains[1].astype(f32)
    for r in range(0, TOK, 16):
        a0, a1 = tok[0, r : r + 16, :].astype(f32), tok[1, r : r + 16, :].astype(f32)
        total = jnp.sum(a0 * a0 + a1 * a1, axis=1, keepdims=True)
        inv = lax.rsqrt(total * (1.0 / D) + EPS)
        hidden[r : r + 16, :1024] = (a0 * inv * g0).astype(bf16)
        hidden[r : r + 16, 1024:] = (a1 * inv * g1).astype(bf16)

    kva["up1"].wait_recv()
    kvs["upf"].start()
    kva["dn1"].wait_recv()
    kvs["dnf"].start()
    for name in ("up2", "dn2"):
        qs[name].start()
    kva["up2"].wait_recv()
    kv_sib[0].start()
    kva["dn2"].wait_recv()
    kv_sib[1].start()

    mine = pl.ds(c * HALF, HALF)
    loads[3].wait()
    key_pre = jnp.dot(hidden[mine, :], wkr[...], preferred_element_type=f32)
    key_pre = jnp.concatenate([key_pre, key_pre], axis=1).astype(bf16).astype(f32)
    key_rope = turned(key_pre, cos_s[mine, :], sin_s[mine, :]).astype(bf16)

    kva["upf"].wait_recv()
    kva["dnf"].wait_recv()
    kv_sib[2].start()
    loads[2].wait()
    for got in kv_sib_got:
        got.wait_recv()
    kv_pre = jnp.dot(hidden[mine, :], wkv[...], preferred_element_type=f32).astype(bf16)
    own0 = (z * NX + x) * HALF
    own1 = SEQ // 2 + (x * NZ + z) * HALF
    own_rows = pl.ds(pl.multiple_of(jnp.where(c == 0, own0, own1), HALF), HALF)
    kv[own_rows, :KR] = scaled_rows(kv_pre.astype(f32), kv_gain[...], KR).astype(bf16)
    kv[own_rows, KR:] = key_rope

    def blk0(zz, xx):
        return kv.at[pl.ds((zz * NX + xx) * HALF, HALF)]

    def blk1(zz, xx):
        return kv.at[pl.ds(SEQ // 2 + (xx * NZ + zz) * HALF, HALF)]

    def first0(i):
        to = lax.rem(x + i, NX)
        return remote(blk0(z, x), blk0(z, x), p1_ss.at[i], p1_rs.at[i], {"sp_1": to})

    def first0_got(i):
        view = blk0(z, lax.rem(x + NX - i, NX))
        return remote(view, view, p1_ss.at[i], p1_rs.at[i], x_up)

    def first1(i):
        to = lax.rem(z + i, NZ)
        return remote(blk1(z, x), blk1(z, x), p1_ss.at[i], p1_rs.at[i], {"sp_0": to})

    def first1_got(i):
        view = blk1(lax.rem(z + NZ - i, NZ), x)
        return remote(view, view, p1_ss.at[i], p1_rs.at[i], z_up)

    @pl.when(c == 0)
    def _():
        for i in (1, 3, 2):
            first0(i).start()

    @pl.when(c == 1)
    def _():
        for i in (1, 7, 2, 6, 3, 5, 4):
            first1(i).start()

    loads[4].wait()
    pool_in[...] = jnp.dot(hidden[...], wpi[...], preferred_element_type=f32).astype(bf16)
    halo_next = remote(pool_in.at[pl.ds(TOK - 16, 16)], halo.at[pl.ds(0, 16)], halo_ss.at[0], halo_rs.at[0], next_dev)
    halo_prev = remote(pool_in.at[pl.ds(0, 16)], halo.at[pl.ds(16, 16)], halo_ss.at[1], halo_rs.at[1], prev_dev)
    halo_next.start()
    halo_prev.start()

    qa["up1"].wait_recv()
    qs["upf"].start()
    qa["dn1"].wait_recv()
    qs["dnf"].start()

    dz = (0, -1, 1, -2, 2, -3, 3, 4)
    dxh = ((0, 0), (0, 1), (-1, 0), (1, 1), (-1, 1), (1, 0), (2, 0), (2, 1))

    def unit_row(cls, n):
        if cls == 0:
            return lax.rem(z + NZ + dz[n], NZ) * UNIT
        dx, h = dxh[n]
        return SEQ // 2 + lax.rem(x + NX + dx, NX) * 2 * UNIT + h * UNIT

    def unit(cls, n):
        return kv.at[pl.ds(unit_row(cls, n), UNIT)]

    def half_unit(n, h):
        return kv.at[pl.ds(unit_row(0, n) + h * (UNIT // 2), UNIT // 2)]

    def ring(src, i, dev):
        return remote(src, src, ring_ss.at[i], ring_rs.at[i], dev)

    def sends_after(cls, n):
        if cls == 0:
            if n == 0:
                return [ring(unit(0, 0), 1, z_up), ring(unit(0, 0), 2, z_down)]
            if n < 5:
                return [ring(unit(0, n), n + 2, z_up if n % 2 else z_down)]
            if n < 7:
                return [ring(half_unit(n, n - 5), n + 2, z_up if n % 2 else z_down)]
            return []
        if n == 0:
            return [
                ring(unit(1, 0), 1, x_up),
                ring(unit(1, 1), 2, x_down),
                ring(unit(1, 1), 3, x_up),
                ring(unit(1, 0), 4, x_down),
            ]
        if n == 2:
            return [ring(unit(1, 2), 5, x_up)]
        if n == 3:
            return [ring(unit(1, 3), 6, x_down)]
        return []

    def arrivals_for(cls, n):
        if cls == 0:
            if n == 7:
                return [ring(half_unit(7, 0), 7, z_up), ring(half_unit(7, 1), 8, z_up)]
            return [ring(unit(0, n), n, z_up)]
        return [ring(unit(1, n), n - 1, x_up)]

    def sib(cls, n):
        return remote(unit(cls, n), unit(cls, n), sib_ss.at[n], sib_rs.at[n], other)

    @pl.when(c == 0)
    def _():
        for i in (1, 3, 2):
            first0_got(i).wait_recv()
        for copy in sends_after(0, 0):
            copy.start()
        sib(0, 0).start()

    @pl.when(c == 1)
    def _():
        for i in (1, 7, 2, 6, 3, 5, 4):
            first1_got(i).wait_recv()
        for copy in sends_after(1, 0):
            copy.start()
        sib(1, 0).start()
        sib(1, 1).start()

    qa["up2"].wait_recv()
    q_sib[0].start()
    qa["dn2"].wait_recv()
    q_sib[1].start()

    remote(halo.at[pl.ds(0, 16)], halo.at[pl.ds(0, 16)], halo_ss.at[0], halo_rs.at[0], next_dev).wait_recv()
    remote(halo.at[pl.ds(16, 16)], halo.at[pl.ds(16, 16)], halo_ss.at[1], halo_rs.at[1], next_dev).wait_recv()
    loads[6].wait()
    loads[7].wait()
    row_i = lax.broadcasted_iota(jnp.int32, (TOK, TOK), 0)
    gap = lax.broadcasted_iota(jnp.int32, (TOK, TOK), 1) - row_i
    rim_row = lax.broadcasted_iota(jnp.int32, (TOK, 32), 0)
    rim_col = lax.broadcasted_iota(jnp.int32, (TOK, 32), 1)
    before = rim_col < 16
    rim_gap = jnp.where(before, rim_col - 16, rim_col - 16 + TOK) - rim_row
    rim_ok = (before & (sp > 0)) | (~before & (sp < NZ * NX - 1))
    place = lax.broadcasted_iota(jnp.int32, (TOK, POOL_GROUP), 0) + sp * TOK
    for g in range(2):
        span = (1 + 3 * c) * (1 + g)
        cols = slice(g * POOL_GROUP, (g + 1) * POOL_GROUP)
        near = ((gap >= -span) & (gap < span)).astype(f32).astype(bf16)
        rim = ((rim_gap >= -span) & (rim_gap < span) & rim_ok).astype(f32).astype(bf16)
        sums = jnp.dot(near, pool_in[:, cols], preferred_element_type=f32)
        sums = sums + jnp.dot(rim, halo[:, cols], preferred_element_type=f32)
        low = jnp.maximum(place - span, 0)
        high = jnp.minimum(place + span, SEQ)
        mean = (sums / (high - low).astype(f32)).astype(bf16)
        spread = (mean.astype(f32) - pool_in[:, cols].astype(f32)).astype(bf16)
        pooled[:, cols] = jnp.dot(spread, mix[g], preferred_element_type=f32).astype(bf16)
    for j in range(4):
        cols = slice(j * 512, (j + 1) * 512)
        out_sum[:, cols] = jnp.dot(pooled[...], wop[:, cols], preferred_element_type=f32)

    qa["upf"].wait_recv()
    qa["dnf"].wait_recv()
    q_sib[2].start()
    loads[5].wait()
    for i in (8, 9, 10):
        loads[i].wait()
    for got in q_sib_got:
        got.wait_recv()
    q_pre = jnp.dot(hidden[...], wq[...], preferred_element_type=f32).astype(bf16)
    q_lat[...] = scaled_rows(q_pre.astype(f32), q_gain[...], QR).astype(bf16)
    q_nope[...] = jnp.dot(q_lat[...], wqn[...], preferred_element_type=f32).astype(bf16)
    q_rot = jnp.dot(q_lat[...], wqr[...], preferred_element_type=f32).astype(bf16).astype(f32)
    lane = lax.broadcasted_iota(jnp.int32, (TOK, 128), 1)
    for h in range(HEADS):
        rows = slice(h * TOK, (h + 1) * TOK)
        if h % 2 == 0:
            pair = turned(q_rot[:, h * 64 : h * 64 + 128], cos_s[...], sin_s[...]) * SCALE
        keep = lane < 64 if h % 2 == 0 else lane >= 64
        q_all[rows, KR:] = jnp.where(keep, pair, 0.0).astype(bf16)
        head = slice(h * NOPE_DIM, (h + 1) * NOPE_DIM)
        absorbed = lax.dot_general(
            q_nope[:, head], wku[:, head], (((1,), (1,)), ((), ())), preferred_element_type=f32
        )
        q_all[rows, :KR] = (absorbed * SCALE).astype(bf16)

    last = 15

    def row_of(i):
        own = (i == 0) | ((lax.rem(i, 2) == 1) & (i < last))
        n = jnp.where(i == 0, 0, jnp.where(i == last, 7, jnp.where(own, (i + 1) // 2, i // 2 - 1)))
        cls = jnp.where(own, c, 1 - c)
        dzn = jnp.where(n == 7, 4, jnp.where(lax.rem(n, 2) == 1, -((n + 1) // 2), (n + 1) // 2))
        row0 = lax.rem(z + NZ + dzn, NZ) * UNIT
        dxn = jnp.where(n < 2, 0, jnp.where(n > 5, 2, jnp.where(lax.rem(n, 2) == 0, -1, 1)))
        hn = jnp.where(
            (n == 1) | (n == 3) | (n == 4) | (n == 7), 1, 0
        )
        row1 = SEQ // 2 + lax.rem(x + NX + dxn, NX) * 2 * UNIT + hn * UNIT
        return pl.multiple_of(jnp.where(cls == 0, row0, row1), UNIT), own, n

    def acquire(i):
        for n in range(1, 8):

            @pl.when((i == 2 * n - 1) & (c == 0))
            def _():
                for copy in arrivals_for(0, n):
                    copy.wait_recv()
                for copy in sends_after(0, n):
                    copy.start()
                sib(0, n).start()

            if n >= 2:

                @pl.when((i == 2 * n - 1) & (c == 1))
                def _():
                    for copy in arrivals_for(1, n):
                        copy.wait_recv()
                    for copy in sends_after(1, n):
                        copy.start()
                    sib(1, n).start()

        at, own, n = row_of(i)

        @pl.when(jnp.logical_not(own))
        def _():
            view = kv.at[pl.ds(at, UNIT)]
            remote(view, view, sib_ss.at[n], sib_rs.at[n], other).wait_recv()

        return at

    def scores(at, h):
        s_scr[h] = lax.dot_general(
            q_all[h * MB : (h + 1) * MB, :], kv[pl.ds(at, UNIT), :], (((1,), (1,)), ((), ())), preferred_element_type=f32
        )

    def softmax(h):
        for r in range(0, MB, SUB):
            g = slice(h * MB + r, h * MB + r + SUB)
            s = [s_scr[h, r : r + SUB, j * 128 : (j + 1) * 128] for j in range(UNIT // 128)]
            m_old = m_s[g, :]
            top = s[0]
            for t in s[1:]:
                top = jnp.maximum(top, t)
            m_new = jnp.maximum(m_old, jnp.max(top, axis=1, keepdims=True))
            alpha = jnp.exp2(m_old - m_new)
            total = l_s[g, :] * alpha
            for j, t in enumerate(s):
                p = jnp.exp2(t - m_new)
                total = total + p
                p_scr[h, r : r + SUB, j * 128 : (j + 1) * 128] = p.astype(bf16)
            m_s[g, :] = m_new
            l_s[g, :] = total
            for j in range(2):
                cols = slice(j * 128, (j + 1) * 128)
                acc[g, cols] = acc[g, cols] * alpha

    def product(at, h):
        g = slice(h * MB, (h + 1) * MB)
        acc[g, :] = acc[g, :] + jnp.dot(p_scr[h], kv[pl.ds(at, UNIT), :KR], preferred_element_type=f32)

    m_s[...] = jnp.full(m_s.shape, -1e30, f32)
    l_s[...] = jnp.zeros(l_s.shape, f32)
    acc[...] = jnp.zeros(acc.shape, f32)
    p_scr[1] = jnp.zeros(p_scr.shape[1:], bf16)
    scores(row_of(jnp.int32(0))[0], 0)

    def step(i, carry):
        now = row_of(i)[0]
        past = row_of(jnp.maximum(i - 1, 0))[0]
        nxt = jnp.minimum(i + 1, last)

        @pl.when(i < last)
        def _():
            acquire(i + 1)

        scores(now, 1)
        softmax(0)
        product(past, 1)
        scores(row_of(nxt)[0], 0)
        softmax(1)
        product(now, 0)
        return carry

    lax.fori_loop(0, last + 1, step, 0)
    product(row_of(jnp.int32(last))[0], 1)

    loads[11].wait()
    loads[12].wait()
    for h in range(HEADS):
        rows = slice(h * TOK, (h + 1) * TOK)
        head = slice(h * VALUE_DIM, (h + 1) * VALUE_DIM)
        total = jnp.sum(l_s[rows, :], axis=1, keepdims=True)
        weighted = (acc[rows, :] / total).astype(bf16)
        att[:, head] = jnp.dot(weighted, wvu[:, head], preferred_element_type=f32).astype(bf16)

    theirs = pl.ds((1 - c) * HALF, HALF)

    def share(j):
        return remote(send_buf.at[j], recv_buf.at[j], out_ss.at[j], out_rs.at[j], other)

    for j in range(4):
        cols = slice(j * 512, (j + 1) * 512)
        out_sum[:, cols] = out_sum[:, cols] + jnp.dot(att[...], woa[:, cols], preferred_element_type=f32)
        send_buf[j] = out_sum[theirs, cols].astype(bf16)
        share(j).start()
    for j in range(4):
        cols = slice(j * 512, (j + 1) * 512)
        share(j).wait_recv()
        out[:, cols] = (out_sum[mine, cols] + recv_buf[j].astype(f32)).astype(bf16)

    tok_copy.wait_send()
    gain_copy.wait_send()
    for group in (kvs, qs):
        for copy in group.values():
            copy.wait_send()
    for copy in kv_sib + q_sib:
        copy.wait_send()
    halo_next.wait_send()
    halo_prev.wait_send()
    for j in range(4):
        share(j).wait_send()

    @pl.when(c == 0)
    def _():
        for i in range(1, NX):
            first0(i).wait_send()
        for n in range(8):
            for copy in sends_after(0, n):
                copy.wait_send()
            sib(0, n).wait_send()

    @pl.when(c == 1)
    def _():
        for i in range(1, NZ):
            first1(i).wait_send()
        for n in range(8):
            for copy in sends_after(1, n):
                copy.wait_send()
            sib(1, n).wait_send()


def on_device(
    tokens,
    norm_gain,
    w_q_down,
    q_gain,
    w_q_nope,
    w_q_rope,
    w_kv_down,
    kv_gain,
    w_k_up,
    w_v_up,
    w_k_rope,
    w_pool_in,
    w_pool_mix,
    w_out_attn,
    w_out_pool,
):
    row_table, col_table = rope_tables()
    anywhere = pl.BlockSpec(memory_space=pl.ANY)
    vmem = pl.BlockSpec(memory_space=pltpu.VMEM)
    dma = pltpu.SemaphoreType.DMA
    result = pl.pallas_call(
        layer_body,
        out_shape=jax.ShapeDtypeStruct((HALF, D), bf16),
        in_specs=[anywhere, anywhere, anywhere, vmem, anywhere, anywhere, anywhere, vmem] + [anywhere] * 7 + [vmem, vmem],
        out_specs=vmem,
        scratch_shapes=[
            pltpu.VMEM((2, TOK, 1024), bf16),
            pltpu.VMEM((2, 1, 1024), bf16),
            pltpu.VMEM((TOK, D), bf16),
            pltpu.VMEM((D, KR), bf16),
            pltpu.VMEM((D, QR), bf16),
            pltpu.VMEM((D, ROPE_DIM), bf16),
            pltpu.VMEM((D, 512), bf16),
            pltpu.VMEM((QR, 1024), bf16),
            pltpu.VMEM((QR, 512), bf16),
            pltpu.VMEM((KR, 1024), bf16),
            pltpu.VMEM((KR, 1024), bf16),
            pltpu.VMEM((2, POOL_GROUP, POOL_GROUP), bf16),
            pltpu.VMEM((1024, D), bf16),
            pltpu.VMEM((512, D), bf16),
            pltpu.VMEM((TOK, 128), f32),
            pltpu.VMEM((TOK, 128), f32),
            pltpu.VMEM((SEQ, WIDE), bf16),
            pltpu.VMEM((ROWS, WIDE), bf16),
            pltpu.VMEM((TOK, QR), bf16),
            pltpu.VMEM((TOK, 1024), bf16),
            pltpu.VMEM((TOK, 512), bf16),
            pltpu.VMEM((32, 512), bf16),
            pltpu.VMEM((TOK, 512), bf16),
            pltpu.VMEM((TOK, D), f32),
            pltpu.VMEM((TOK, 1024), bf16),
            pltpu.VMEM((4, HALF, 512), bf16),
            pltpu.VMEM((4, HALF, 512), bf16),
            pltpu.VMEM((2, MB, UNIT), f32),
            pltpu.VMEM((2, MB, UNIT), bf16),
            pltpu.VMEM((ROWS, KR), f32),
            pltpu.VMEM((ROWS, 128), f32),
            pltpu.VMEM((ROWS, 128), f32),
            dma((13,)),
            dma((2,)),
            dma((2,)),
            dma((2, 6)),
            dma((2, 6)),
            dma((2, 3)),
            dma((2, 3)),
            dma((8,)),
            dma((8,)),
            dma((9,)),
            dma((9,)),
            dma((8,)),
            dma((8,)),
            dma((2,)),
            dma((2,)),
            dma((4,)),
            dma((4,)),
        ],
        compiler_params=pltpu.CompilerParams(
            collective_id=0, has_side_effects=True, vmem_limit_bytes=60 * 2**20
        ),
    )(
        tokens[0],
        norm_gain[None],
        w_q_down,
        q_gain[None],
        w_q_nope,
        w_q_rope,
        w_kv_down,
        kv_gain[None],
        w_k_up,
        w_v_up,
        w_k_rope,
        w_pool_in,
        w_pool_mix,
        w_out_attn,
        w_out_pool,
        jnp.asarray(row_table),
        jnp.asarray(col_table),
    )
    return result[None]


def solution(mesh):
    torus = Mesh(
        mesh.devices.reshape(NZ, NX, mesh.shape["fs"], mesh.shape["tp"]), ("sp_0", "sp_1", "fs", "tp")
    )
    placed = (
        P("fs", SP, "tp"),
        P("tp"),
        P("fs", None),
        P(),
        P(None, "tp"),
        P(None, "tp"),
        P("fs", None),
        P(),
        P(None, "tp"),
        P(None, "tp"),
        P(),
        P(None, "tp"),
        P(),
        P("tp", None),
        P("tp", None),
    )
    return jax.shard_map(
        on_device, mesh=torus, in_specs=placed, out_specs=P("fs", SP_TP, None), check_vma=False
    )
```

time: 170 us -> 78.6 us (0.46)
  waiting for transfers between devices: 84.3 us -> 0 us
  Pallas kernels: 23.2 us -> 73.4 us
  blocking collectives: 24.1 us -> 0 us
  between operations: 13.8 us -> 0.01 us
  matrix products: 11.8 us -> 0 us
  other arithmetic: 5.35 us -> 0 us
  starting transfers between devices: 2.99 us -> 0 us
    all_gather x2 -> x0, waiting for transfers between devices: 81.5 us -> none  [the longest x1 44.7 us: gathered_by_axis(): out = lax.all_gather(out, axes[number], axis=dim, tiled=True)]
    pallas_call x1, Pallas kernels: 23.2 us -> 73.4 us  [on_device(): pl.pallas_call(layer_body, out_shape=jax.ShapeDtypeStruct((HALF, D), bf16...]
    all_gather x3 -> x0, blocking collectives: 19.3 us -> none  [the longest x1 12.2 us: gathered_by_axis(): out = lax.all_gather(out, axes[number], axis=dim, tiled=True)]
    dot_general x11 -> x0, matrix products: 11.8 us -> none  [the longest x1 2.22 us: on_device(): jnp.dot(hidden, w_pool_in, preferred_element_type=jnp.float32)]
    all_to_all x1 -> x0, blocking collectives: 4.83 us -> none  [summed_on_arrival(): lax.all_to_all(tiles, axis, split_axis=0, concat_axis=0, tiled=True)]
    ppermute x2 -> x0, starting transfers between devices: 2.94 us -> none  [the longest x1 1.65 us: padded_2(): before = lax.ppermute(last, axis, up)]
    ppermute x2 -> x0, waiting for transfers between devices: 2.74 us -> none  [the longest x1 2.74 us: padded_2(): after = lax.ppermute(first, axis, down)]
    concatenate x3 -> x0, other arithmetic: 2.52 us -> none  [the longest x1 2.22 us: sent_together(): both = jnp.concatenate(arrays, axis=along)]
  transfers between devices with their start and end apart: 4 -> 0, of which waited for: 3 -> 0; matrix products, arithmetic and copies ran while one was open for 7% -> 0% of each run, Pallas kernels for 0% -> 0%
where the time goes in v2:
time: 78.6 us; the launch traced here: 78.4 us
  Pallas kernels  73.4 us (93%)
  local copies, waits for them, and re-layouts  4.99 us (6%)
    pallas_call x1, Pallas kernels, on_device(): pl.pallas_call(layer_body, out_shape=jax.ShapeDtypeStruct((HALF, D), bf16...  73.4 us
    unnamed x2, local copies, waits for them, and re-layouts  3.72 us

profile of v2, /device:TPU:1, one launch (start us, length us, event | category | flops | bytes accessed | tf_op | source)
XLA Modules:
  0.0 78.4 jit_solution(14050002367166992557)
XLA Ops:
  0.0 1.3 %broadcast_in_dim.12.norm_gain = bf16[1,1024]{1,0:T(2,128)(2,1)} reshape(bf16[1024]{0:T(1024)(128)(2,1)} %param.18) | data formatting | bytes 4096 | tf_op jit(solution)/shard_map/broadcast_in_dim | solution.py:692
  1.3 1.9 %copy.18.w_k_rope = bf16[2048,64]{1,0:T(8,128)(2,1)} copy(bf16[2048,64]{0,1:T(8,128)(2,1)} %param.27) | data formatting | bytes 524288 | tf_op args[10]
  3.2 73.4 %shard_map.163 = bf16[96,2048]{1,0:T(8,128)(2,1)} custom-call(bf16[192,1024]{1,0:T(8,128)(2,1)} %bitcast.5, bf16[1,1024]{1,0:T(2,128)(2,1)} %broadcast_in_dim.12.norm_gain, bf16[512,512]{1,0:T(8,128)(2,1)} %w_q_down.1, f32[1,512]{1,0:T(1,128)} %bitcast.6, bf16[512,1024]{1,0:T(8,128)(2,1)} %w_q_nope.1, bf16[512,512]{1,0:T(8,128)(2,1)} %w_q_rope.1, ...), custom_call_target="tpu_custom_call" | custom-call | tf_op jit(solution)/shard_map/pallas_call | solution.py:631
  76.6 1.8 %copy.20 = bf16[1,96,2048]{2,1,0:T(8,128)(2,1)} copy(bf16[1,96,2048]{2,1,0:T(8,128)(2,1)} %bitcast.4) | data formatting | bytes 786432

commit v3 on v2

v3 whole, which is shorter than its diff:
```python
import functools

import jax
import jax.numpy as jnp
import numpy as np
from jax import lax
from jax.experimental import pallas as pl
from jax.experimental.pallas import tpu as pltpu
from jax.sharding import Mesh
from jax.sharding import PartitionSpec as P

NOPE_DIM = 128
ROPE_DIM = 64
VALUE_DIM = 128
GRID_W = 64
POOL_GROUP = 256
SP = ("sp_0", "sp_1")
SP_TP = ("sp_0", "sp_1", "tp")
EPS = 1e-06
THETA = 10000.0
LOG2E = 1.4426950408889634
MESH = pl.DeviceIdType.MESH

NZ, NX, NY = 8, 4, 4
TOK = 192
HALF = 96
D = 2048
HEADS = 8
QR, KR = 512, 256
WIDE = 384
UNIT = 384
ROWS = HEADS * TOK
MB = 384
STEP = 2 * UNIT
SUB = 32
SEQ = NZ * NX * TOK
SCALE = (NOPE_DIM + ROPE_DIM) ** (-0.5) * LOG2E
f32, bf16 = jnp.float32, jnp.bfloat16


def rope_tables():
    inverse = (THETA ** (-np.arange(0, ROPE_DIM // 2, 2) / (ROPE_DIM // 2))).astype(np.float32)
    lane = np.arange(128)
    freq = inverse[lane % 16]
    by_row = (lane // 32) % 2 == 0
    sign = np.where((lane // 16) % 2 == 0, -1.0, 1.0)

    def table(count, keep):
        angle = (np.arange(count, dtype=np.float32)[:, None] * freq).astype(np.float64)
        cos = np.where(keep, np.cos(angle), 0.0)
        sin = np.where(keep, np.sin(angle) * sign, 0.0)
        return np.stack([cos, sin]).astype(np.float32)

    return table(SEQ // GRID_W, by_row), table(GRID_W, ~by_row)


def turned(values, cos, sin):
    lane = lax.broadcasted_iota(jnp.int32, values.shape, 1)
    ahead = pltpu.roll(values, 112, 1)
    behind = pltpu.roll(values, 16, 1)
    partner = jnp.where((lane // 16) % 2 == 0, ahead, behind)
    return values * cos + partner * sin


def scaled_rows(values, gain, width):
    mean = jnp.sum(values * values, axis=1, keepdims=True) * (1.0 / width)
    return values * lax.rsqrt(mean + EPS) * gain


def layer_body(
    tokens,
    norm_gain,
    w_q_down,
    q_gain,
    w_q_nope,
    w_q_rope,
    w_kv_down,
    kv_gain,
    w_k_up,
    w_v_up,
    w_k_rope,
    w_pool_in,
    w_pool_mix,
    w_out_attn,
    w_out_pool,
    row_hbm,
    col_hbm,
    out,
    tok,
    gains,
    q_gain_s,
    kv_gain_s,
    row_table,
    col_table,
    hidden,
    wkv,
    wq,
    wkr,
    wpi,
    wqn,
    wqr,
    wku,
    wvu,
    mix,
    woa,
    wop,
    cos_s,
    sin_s,
    kv,
    q_all,
    q_lat,
    q_nope,
    pool_in,
    halo,
    pooled,
    out_sum,
    att,
    send_buf,
    recv_buf,
    s_scr,
    p_scr,
    acc,
    m_s,
    l_s,
    loc,
    tok_ss,
    tok_rs,
    w_ss,
    w_rs,
    ws_ss,
    ws_rs,
    p1_ss,
    p1_rs,
    ring_ss,
    ring_rs,
    sib_ss,
    sib_rs,
    halo_ss,
    halo_rs,
    out_ss,
    out_rs,
):
    z, x = lax.axis_index("sp_0"), lax.axis_index("sp_1")
    y, c = lax.axis_index("fs"), lax.axis_index("tp")
    sp = z * NX + x
    other = {"tp": 1 - c}
    y_up, y_down = {"fs": lax.rem(y + 1, NY)}, {"fs": lax.rem(y + NY - 1, NY)}
    z_up, z_down = {"sp_0": lax.rem(z + 1, NZ)}, {"sp_0": lax.rem(z + NZ - 1, NZ)}
    x_up, x_down = {"sp_1": lax.rem(x + 1, NX)}, {"sp_1": lax.rem(x + NX - 1, NX)}
    sp_next, sp_prev = lax.rem(sp + 1, NZ * NX), lax.rem(sp + NZ * NX - 1, NZ * NX)
    next_dev = {"sp_0": sp_next // NX, "sp_1": sp_next % NX}
    prev_dev = {"sp_0": sp_prev // NX, "sp_1": sp_prev % NX}

    def remote(src, dst, ssem, rsem, dev):
        return pltpu.make_async_remote_copy(
            src_ref=src, dst_ref=dst, send_sem=ssem, recv_sem=rsem, device_id=dev, device_id_type=MESH
        )

    barrier = pltpu.get_barrier_semaphore()
    partners = [other, y_up, y_down, next_dev, prev_dev]
    partners += [{"sp_0": lax.rem(z + i, NZ)} for i in range(1, NZ)]
    partners += [{"sp_1": lax.rem(x + i, NX)} for i in range(1, NX)]
    for dev in partners:
        pl.semaphore_signal(barrier, inc=1, device_id=dev, device_id_type=MESH)

    def local(i, src, dst):
        return pltpu.make_async_copy(src, dst, loc.at[i])

    loads = [
        local(0, tokens, tok.at[c]),
        local(1, norm_gain, gains.at[c]),
        local(2, w_kv_down, wkv.at[pl.ds(y * 512, 512)]),
        local(3, w_k_rope, wkr),
        local(4, w_pool_in, wpi),
        local(5, w_q_down, wq.at[pl.ds(y * 512, 512)]),
        local(6, w_pool_mix.at[pl.ds(2 * c, 2)], mix),
        local(7, w_out_pool, wop),
        local(8, w_q_nope, wqn),
        local(9, w_q_rope, wqr),
        local(10, w_k_up, wku),
        local(11, w_v_up, wvu),
        local(12, w_out_attn, woa),
        local(13, q_gain, q_gain_s),
        local(14, kv_gain, kv_gain_s),
        local(15, row_hbm, row_table),
        local(16, col_hbm, col_table),
    ]
    for i in (0, 1, 2, 15, 16, 5):
        loads[i].start()

    m_s[...] = jnp.full(m_s.shape, -1e30, f32)
    l_s[...] = jnp.zeros(l_s.shape, f32)
    acc[...] = jnp.zeros(acc.shape, f32)
    pl.semaphore_wait(barrier, len(partners))

    tok_copy = remote(tok.at[c], tok.at[c], tok_ss.at[0], tok_rs.at[0], other)
    gain_copy = remote(gains.at[c], gains.at[c], tok_ss.at[1], tok_rs.at[1], other)
    loads[0].wait()
    loads[1].wait()
    tok_copy.start()
    gain_copy.start()

    y1, y2, y3 = lax.rem(y + 3, NY), lax.rem(y + 1, NY), lax.rem(y + 2, NY)

    def weight_copies(w, buf, base, part):
        def rows(of, p):
            return buf.at[pl.ds(of * 512 + base + p * part, part)]

        ss, rs = w_ss.at[w], w_rs.at[w]

        def copy(i, of, p, dev):
            return remote(rows(of, p), rows(of, p), ss.at[i], rs.at[i], dev)

        def sends(name):
            return {
                "up1": lambda: copy(0, y, 0, y_up),
                "up2": lambda: copy(1, y, 1, y_up),
                "dn1": lambda: copy(2, y, 1, y_down),
                "dn2": lambda: copy(3, y, 0, y_down),
                "upf": lambda: copy(4, y1, 0, y_up),
                "dnf": lambda: copy(5, y2, 1, y_down),
            }[name]()

        def got(name):
            return {
                "up1": lambda: copy(0, y1, 0, y_up),
                "up2": lambda: copy(1, y1, 1, y_up),
                "dn1": lambda: copy(2, y2, 1, y_up),
                "dn2": lambda: copy(3, y2, 0, y_up),
                "upf": lambda: copy(4, y3, 0, y_up),
                "dnf": lambda: copy(5, y3, 1, y_up),
            }[name]()

        return sends, got

    def weight_sibling(w, buf, base, count, i):
        view = buf.at[pl.ds((y1, y2, y3)[i] * 512 + base, count)]
        return remote(view, view, ws_ss.at[w, i], ws_rs.at[w, i], other)

    kv_send, kv_got = weight_copies(0, wkv, 0, 256)
    q_send, q_got = weight_copies(1, wq, c * 256, 128)

    def kv_sib(i):
        return weight_sibling(0, wkv, 0, 512, i)

    def q_sib(i):
        return weight_sibling(1, wq, c * 256, 256, i)

    def q_sib_got(i):
        return weight_sibling(1, wq, (1 - c) * 256, 256, i)

    def start_queries():
        for name in ("up1", "dn1", "up2", "dn2"):
            q_send(name).start()

    loads[2].wait()

    @pl.when(c == 1)
    def _():
        for name in ("up1", "dn1", "up2", "dn2"):
            kv_send(name).start()

    for i in (3, 4, 6, 7, 8, 9, 10, 11, 13, 14, 12):
        loads[i].start()
    loads[5].wait()

    loads[15].wait()
    loads[16].wait()
    for k in range(TOK // GRID_W):
        rows = slice(k * GRID_W, (k + 1) * GRID_W)
        at = 3 * sp + k
        cos_s[rows, :] = row_table[0, pl.ds(at, 1), :] + col_table[0]
        sin_s[rows, :] = row_table[1, pl.ds(at, 1), :] + col_table[1]

    remote(tok.at[1 - c], tok.at[1 - c], tok_ss.at[0], tok_rs.at[0], other).wait_recv()
    remote(gains.at[1 - c], gains.at[1 - c], tok_ss.at[1], tok_rs.at[1], other).wait_recv()
    gain = [gains[half].astype(f32) for half in range(2)]
    for r in range(0, TOK, 16):
        parts = [tok[half, r : r + 16, :].astype(f32) for half in range(2)]
        total = jnp.sum(parts[0] * parts[0] + parts[1] * parts[1], axis=1, keepdims=True)
        inv = lax.rsqrt(total * (1.0 / D) + EPS)
        for half in range(2):
            for j in range(8):
                cols = slice(j * 128, (j + 1) * 128)
                at = half * 1024 + j * 128
                hidden[r : r + 16, at : at + 128] = (parts[half][:, cols] * inv * gain[half][j : j + 1, :]).astype(bf16)
    @pl.when(c == 1)
    def _():
        kv_got("up1").wait_recv()
        kv_send("upf").start()
        kv_got("dn1").wait_recv()
        kv_send("dnf").start()
        start_queries()
        kv_got("up2").wait_recv()
        kv_sib(0).start()
        kv_got("dn2").wait_recv()
        kv_sib(1).start()

    @pl.when(c == 0)
    def _():
        kv_sib(0).wait_recv()
        start_queries()
        kv_sib(1).wait_recv()

    loads[4].wait()
    pool_in[...] = jnp.dot(hidden[...], wpi[...], preferred_element_type=f32).astype(bf16)
    halo_next = remote(pool_in.at[pl.ds(TOK - 16, 16)], halo.at[pl.ds(0, 16)], halo_ss.at[0], halo_rs.at[0], next_dev)
    halo_prev = remote(pool_in.at[pl.ds(0, 16)], halo.at[pl.ds(16, 16)], halo_ss.at[1], halo_rs.at[1], prev_dev)
    halo_next.start()
    halo_prev.start()

    mine = pl.ds(c * HALF, HALF)
    loads[3].wait()
    key_pre = lax.dot_general(
        hidden[mine, :], wkr[...], (((1,), (1,)), ((), ())), preferred_element_type=f32
    )
    key_pre = jnp.concatenate([key_pre, key_pre], axis=1).astype(bf16).astype(f32)
    key_rope = turned(key_pre, cos_s[mine, :], sin_s[mine, :]).astype(bf16)

    @pl.when(c == 1)
    def _():
        kv_got("upf").wait_recv()
        kv_got("dnf").wait_recv()
        kv_sib(2).start()

    @pl.when(c == 0)
    def _():
        kv_sib(2).wait_recv()

    loads[14].wait()
    kv_pre = jnp.dot(hidden[mine, :], wkv[...], preferred_element_type=f32).astype(bf16)
    own0 = x * HALF
    own1 = SEQ // 2 + z * HALF
    own_rows = pl.ds(pl.multiple_of(jnp.where(c == 0, own0, own1), HALF), HALF)
    kv[own_rows, :KR] = scaled_rows(kv_pre.astype(f32), kv_gain_s[...], KR).astype(bf16)
    kv[own_rows, KR:] = key_rope

    def blk0(xx):
        return kv.at[pl.ds(xx * HALF, HALF)]

    def blk1(zz):
        return kv.at[pl.ds(SEQ // 2 + zz * HALF, HALF)]

    def first0(i):
        to = lax.rem(x + i, NX)
        return remote(blk0(x), blk0(x), p1_ss.at[i], p1_rs.at[i], {"sp_1": to})

    def first0_got(i):
        view = blk0(lax.rem(x + NX - i, NX))
        return remote(view, view, p1_ss.at[i], p1_rs.at[i], x_up)

    def first1(i):
        to = lax.rem(z + i, NZ)
        return remote(blk1(z), blk1(z), p1_ss.at[i], p1_rs.at[i], {"sp_0": to})

    def first1_got(i):
        view = blk1(lax.rem(z + NZ - i, NZ))
        return remote(view, view, p1_ss.at[i], p1_rs.at[i], z_up)

    @pl.when(c == 0)
    def _():
        for i in (1, 3, 2):
            first0(i).start()

    @pl.when(c == 1)
    def _():
        for i in (1, 7, 2, 6, 3, 5, 4):
            first1(i).start()

    q_got("up1").wait_recv()
    q_send("upf").start()
    q_got("dn1").wait_recv()
    q_send("dnf").start()

    def unit(cls, n):
        return kv.at[pl.ds(cls * (SEQ // 2) + n * UNIT, UNIT)]

    def half_unit(n, h):
        return kv.at[pl.ds(n * UNIT + h * (UNIT // 2), UNIT // 2)]

    def ring(src, dst, i, dev):
        return remote(src, dst, ring_ss.at[i], ring_rs.at[i], dev)

    def sends_after(cls, n):
        if cls == 0:
            up, down = z_up, z_down
            if n == 0:
                return [ring(unit(0, 0), unit(0, 1), 1, up), ring(unit(0, 0), unit(0, 2), 2, down)]
            if n < 5:
                return [ring(unit(0, n), unit(0, n + 2), n + 2, up if n % 2 else down)]
            if n < 7:
                return [ring(half_unit(n, n - 5), half_unit(7, n - 5), n + 2, up if n % 2 else down)]
            return []
        up, down = x_up, x_down
        if n == 0:
            return [
                ring(unit(1, 0), unit(1, 2), 2, up),
                ring(unit(1, 1), unit(1, 3), 3, down),
                ring(unit(1, 1), unit(1, 4), 4, up),
                ring(unit(1, 0), unit(1, 5), 5, down),
            ]
        if n == 2:
            return [ring(unit(1, 2), unit(1, 6), 6, up)]
        if n == 3:
            return [ring(unit(1, 3), unit(1, 7), 7, down)]
        return []

    def arrivals_for(cls, n):
        if cls == 0 and n == 7:
            return [ring(half_unit(7, h), half_unit(7, h), 7 + h, z_up) for h in range(2)]
        return [ring(unit(cls, n), unit(cls, n), n, z_up)]

    def sib(cls, n):
        return remote(unit(cls, n), unit(cls, n), sib_ss.at[n], sib_rs.at[n], other)

    def acquire_own(cls, n):
        for copy in arrivals_for(cls, n):
            copy.wait_recv()
        for copy in sends_after(cls, n):
            copy.start()
        sib(cls, n).start()

    q_got("up2").wait_recv()
    q_sib(0).start()
    q_got("dn2").wait_recv()
    q_sib(1).start()

    @pl.when(c == 0)
    def _():
        for i in (1, 3, 2):
            first0_got(i).wait_recv()
        for copy in sends_after(0, 0):
            copy.start()
        sib(0, 0).start()


    remote(halo.at[pl.ds(0, 16)], halo.at[pl.ds(0, 16)], halo_ss.at[0], halo_rs.at[0], next_dev).wait_recv()
    remote(halo.at[pl.ds(16, 16)], halo.at[pl.ds(16, 16)], halo_ss.at[1], halo_rs.at[1], next_dev).wait_recv()
    loads[6].wait()
    loads[7].wait()
    row_i = lax.broadcasted_iota(jnp.int32, (TOK, TOK), 0)
    gap = lax.broadcasted_iota(jnp.int32, (TOK, TOK), 1) - row_i
    rim_row = lax.broadcasted_iota(jnp.int32, (TOK, 32), 0)
    rim_col = lax.broadcasted_iota(jnp.int32, (TOK, 32), 1)
    before = rim_col < 16
    rim_gap = jnp.where(before, rim_col - 16, rim_col - 16 + TOK) - rim_row
    rim_ok = (before & (sp > 0)) | (~before & (sp < NZ * NX - 1))
    place = lax.broadcasted_iota(jnp.int32, (TOK, POOL_GROUP), 0) + sp * TOK
    for g in range(2):
        span = (1 + 3 * c) * (1 + g)
        cols = slice(g * POOL_GROUP, (g + 1) * POOL_GROUP)
        near = ((gap >= -span) & (gap < span)).astype(f32).astype(bf16)
        rim = ((rim_gap >= -span) & (rim_gap < span) & rim_ok).astype(f32).astype(bf16)
        sums = jnp.dot(near, pool_in[:, cols], preferred_element_type=f32)
        sums = sums + jnp.dot(rim, halo[:, cols], preferred_element_type=f32)
        low = jnp.maximum(place - span, 0)
        high = jnp.minimum(place + span, SEQ)
        mean = (sums / (high - low).astype(f32)).astype(bf16)
        spread = (mean.astype(f32) - pool_in[:, cols].astype(f32)).astype(bf16)
        pooled[:, cols] = jnp.dot(spread, mix[g], preferred_element_type=f32).astype(bf16)
    for j in range(4):
        cols = slice(j * 512, (j + 1) * 512)
        out_sum[:, cols] = jnp.dot(pooled[...], wop[:, cols], preferred_element_type=f32)

    q_got("upf").wait_recv()
    q_got("dnf").wait_recv()
    q_sib(2).start()
    for i in (8, 9, 10, 13):
        loads[i].wait()
    for i in range(3):
        q_sib_got(i).wait_recv()
    q_pre = jnp.dot(hidden[...], wq[...], preferred_element_type=f32).astype(bf16)
    q_lat[...] = scaled_rows(q_pre.astype(f32), q_gain_s[...], QR).astype(bf16)
    q_nope[...] = jnp.dot(q_lat[...], wqn[...], preferred_element_type=f32).astype(bf16)
    q_rot = jnp.dot(q_lat[...], wqr[...], preferred_element_type=f32).astype(bf16).astype(f32)
    lane = lax.broadcasted_iota(jnp.int32, (TOK, 128), 1)
    for h in range(HEADS):
        rows = slice(h * TOK, (h + 1) * TOK)
        if h % 2 == 0:
            pair = turned(q_rot[:, h * 64 : h * 64 + 128], cos_s[...], sin_s[...]) * SCALE
        keep = lane < 64 if h % 2 == 0 else lane >= 64
        q_all[rows, KR:] = jnp.where(keep, pair, 0.0).astype(bf16)
        head = slice(h * NOPE_DIM, (h + 1) * NOPE_DIM)
        absorbed = lax.dot_general(
            q_nope[:, head], wku[:, head], (((1,), (1,)), ((), ())), preferred_element_type=f32
        )
        q_all[rows, :KR] = (absorbed * SCALE).astype(bf16)

    @pl.when(c == 0)
    def _():
        acquire_own(0, 1)
        acquire_own(0, 2)

    @pl.when(c == 1)
    def _():
        for i in (1, 7, 2, 6, 3, 5, 4):
            first1_got(i).wait_recv()
        for copy in sends_after(1, 0):
            copy.start()
        sib(1, 0).start()
        sib(1, 1).start()

    steps = 2 * (SEQ // 2) // STEP

    def row_of(i):
        cls = lax.rem(i + c, 2)
        return pl.multiple_of(cls * (SEQ // 2) + (i // 2) * STEP, STEP)

    def acquire(i):
        for m in range(1, 4):
            for cls in range(2):

                @pl.when((i == 2 * m) & (c == cls))
                def _():
                    for n in (2 * m, 2 * m + 1):
                        if n > 2 or cls == 1:
                            acquire_own(cls, n)

        @pl.when(lax.rem(i, 2) == 1)
        def _():
            for n in range(2):
                at = (1 - c) * (SEQ // 2) + (i // 2) * STEP + n * UNIT
                view = kv.at[pl.ds(at, UNIT)]
                remote(view, view, sib_ss.at[i - 1 + n], sib_rs.at[i - 1 + n], other).wait_recv()

    def scores(i, h):
        s_scr[h % 2] = lax.dot_general(
            q_all[h * MB : (h + 1) * MB, :],
            kv[pl.ds(row_of(i), STEP), :],
            (((1,), (1,)), ((), ())),
            preferred_element_type=f32,
        )

    def softmax(h):
        for r in range(0, MB, SUB):
            g = slice(h * MB + r, h * MB + r + SUB)
            s = [s_scr[h % 2, r : r + SUB, j * 128 : (j + 1) * 128] for j in range(STEP // 128)]
            m_old = m_s[g, :]
            top = s[0]
            for t in s[1:]:
                top = jnp.maximum(top, t)
            m_new = jnp.maximum(m_old, jnp.max(top, axis=1, keepdims=True))
            alpha = jnp.exp2(m_old - m_new)
            total = l_s[g, :] * alpha
            for j, t in enumerate(s):
                p = jnp.exp2(t - m_new)
                total = total + p
                p_scr[h % 2, r : r + SUB, j * 128 : (j + 1) * 128] = p.astype(bf16)
            m_s[g, :] = m_new
            l_s[g, :] = total
            for j in range(2):
                cols = slice(j * 128, (j + 1) * 128)
                acc[g, cols] = acc[g, cols] * alpha

    def product(i, h):
        g = slice(h * MB, (h + 1) * MB)
        acc[g, :] = acc[g, :] + jnp.dot(p_scr[h % 2], kv[pl.ds(row_of(i), STEP), :KR], preferred_element_type=f32)

    chunks = ROWS // MB
    zero = jnp.int32(0)
    scores(zero, 0)
    for h in range(chunks - 1):
        scores(zero, h + 1)
        softmax(h)
        if h > 0:
            product(zero, h - 1)

    def step(i, carry):
        acquire(i + 1)
        scores(i + 1, 0)
        softmax(chunks - 1)
        product(i, chunks - 2)
        for h in range(chunks - 1):
            scores(i + 1, h + 1)
            softmax(h)
            if h == 0:
                product(i, chunks - 1)
            else:
                product(i + 1, h - 1)
        return carry

    lax.fori_loop(0, steps - 1, step, 0)
    end = jnp.int32(steps - 1)
    softmax(chunks - 1)
    product(end, chunks - 2)
    product(end, chunks - 1)

    loads[11].wait()
    loads[12].wait()
    for h in range(HEADS):
        rows = slice(h * TOK, (h + 1) * TOK)
        head = slice(h * VALUE_DIM, (h + 1) * VALUE_DIM)
        total = jnp.sum(l_s[rows, :], axis=1, keepdims=True)
        weighted = (acc[rows, :] / total).astype(bf16)
        att[:, head] = jnp.dot(weighted, wvu[:, head], preferred_element_type=f32).astype(bf16)

    theirs = pl.ds((1 - c) * HALF, HALF)

    def share(j):
        return remote(send_buf.at[j], recv_buf.at[j], out_ss.at[j], out_rs.at[j], other)

    for j in range(4):
        cols = slice(j * 512, (j + 1) * 512)
        out_sum[:, cols] = out_sum[:, cols] + jnp.dot(att[...], woa[:, cols], preferred_element_type=f32)
        send_buf[j] = out_sum[theirs, cols].astype(bf16)
        share(j).start()
    for j in range(4):
        cols = slice(j * 512, (j + 1) * 512)
        share(j).wait_recv()
        out[:, cols] = (out_sum[mine, cols] + recv_buf[j].astype(f32)).astype(bf16)

    tok_copy.wait_send()
    gain_copy.wait_send()
    for name in ("up1", "up2", "dn1", "dn2", "upf", "dnf"):
        q_send(name).wait_send()
    for i in range(3):
        q_sib(i).wait_send()
    halo_next.wait_send()
    halo_prev.wait_send()
    for j in range(4):
        share(j).wait_send()

    @pl.when(c == 0)
    def _():
        for i in range(1, NX):
            first0(i).wait_send()
        for n in range(8):
            for copy in sends_after(0, n):
                copy.wait_send()
            sib(0, n).wait_send()

    @pl.when(c == 1)
    def _():
        for name in ("up1", "up2", "dn1", "dn2", "upf", "dnf"):
            kv_send(name).wait_send()
        for i in range(3):
            kv_sib(i).wait_send()
        for i in range(1, NZ):
            first1(i).wait_send()
        for n in range(8):
            for copy in sends_after(1, n):
                copy.wait_send()
            sib(1, n).wait_send()


def on_device(
    tokens,
    norm_gain,
    w_q_down,
    q_gain,
    w_q_nope,
    w_q_rope,
    w_kv_down,
    kv_gain,
    w_k_up,
    w_v_up,
    w_k_rope,
    w_pool_in,
    w_pool_mix,
    w_out_attn,
    w_out_pool,
):
    row_table, col_table = rope_tables()
    anywhere = pl.BlockSpec(memory_space=pl.ANY)
    vmem = pl.BlockSpec(memory_space=pltpu.VMEM)
    dma = pltpu.SemaphoreType.DMA
    result = pl.pallas_call(
        layer_body,
        out_shape=jax.ShapeDtypeStruct((HALF, D), bf16),
        in_specs=[anywhere] * 17,
        out_specs=vmem,
        scratch_shapes=[
            pltpu.VMEM((2, TOK, 1024), bf16),
            pltpu.VMEM((2, 8, 128), bf16),
            pltpu.VMEM((1, QR), f32),
            pltpu.VMEM((1, KR), f32),
            pltpu.VMEM((2, SEQ // GRID_W, 128), f32),
            pltpu.VMEM((2, GRID_W, 128), f32),
            pltpu.VMEM((TOK, D), bf16),
            pltpu.VMEM((D, KR), bf16),
            pltpu.VMEM((D, QR), bf16),
            pltpu.VMEM((ROPE_DIM, D), bf16),
            pltpu.VMEM((D, 512), bf16),
            pltpu.VMEM((QR, 1024), bf16),
            pltpu.VMEM((QR, 512), bf16),
            pltpu.VMEM((KR, 1024), bf16),
            pltpu.VMEM((KR, 1024), bf16),
            pltpu.VMEM((2, POOL_GROUP, POOL_GROUP), bf16),
            pltpu.VMEM((1024, D), bf16),
            pltpu.VMEM((512, D), bf16),
            pltpu.VMEM((TOK, 128), f32),
            pltpu.VMEM((TOK, 128), f32),
            pltpu.VMEM((SEQ, WIDE), bf16),
            pltpu.VMEM((ROWS, WIDE), bf16),
            pltpu.VMEM((TOK, QR), bf16),
            pltpu.VMEM((TOK, 1024), bf16),
            pltpu.VMEM((TOK, 512), bf16),
            pltpu.VMEM((32, 512), bf16),
            pltpu.VMEM((TOK, 512), bf16),
            pltpu.VMEM((TOK, D), f32),
            pltpu.VMEM((TOK, 1024), bf16),
            pltpu.VMEM((4, HALF, 512), bf16),
            pltpu.VMEM((4, HALF, 512), bf16),
            pltpu.VMEM((2, MB, STEP), f32),
            pltpu.VMEM((2, MB, STEP), bf16),
            pltpu.VMEM((ROWS, KR), f32),
            pltpu.VMEM((ROWS, 128), f32),
            pltpu.VMEM((ROWS, 128), f32),
            dma((17,)),
            dma((2,)),
            dma((2,)),
            dma((2, 6)),
            dma((2, 6)),
            dma((2, 3)),
            dma((2, 3)),
            dma((8,)),
            dma((8,)),
            dma((9,)),
            dma((9,)),
            dma((8,)),
            dma((8,)),
            dma((2,)),
            dma((2,)),
            dma((4,)),
            dma((4,)),
        ],
        compiler_params=pltpu.CompilerParams(
            collective_id=0, has_side_effects=True, vmem_limit_bytes=60 * 2**20
        ),
    )(
        tokens[0],
        norm_gain.reshape(8, 128),
        w_q_down,
        q_gain[None],
        w_q_nope,
        w_q_rope,
        w_kv_down,
        kv_gain[None],
        w_k_up,
        w_v_up,
        w_k_rope.T,
        w_pool_in,
        w_pool_mix,
        w_out_attn,
        w_out_pool,
        jnp.asarray(row_table),
        jnp.asarray(col_table),
    )
    return result[None]


def solution(mesh):
    torus = Mesh(
        mesh.devices.reshape(NZ, NX, mesh.shape["fs"], mesh.shape["tp"]), ("sp_0", "sp_1", "fs", "tp")
    )
    placed = (
        P("fs", SP, "tp"),
        P("tp"),
        P("fs", None),
        P(),
        P(None, "tp"),
        P(None, "tp"),
        P("fs", None),
        P(),
        P(None, "tp"),
        P(None, "tp"),
        P(),
        P(None, "tp"),
        P(),
        P("tp", None),
        P("tp", None),
    )
    return jax.shard_map(
        on_device, mesh=torus, in_specs=placed, out_specs=P("fs", SP_TP, None), check_vma=False
    )
```

time: 78.6 us -> 63 us (0.80)
  Pallas kernels: 73.4 us -> 61.1 us
  local copies, waits for them, and re-layouts: 4.99 us -> 1.77 us
    pallas_call x1, Pallas kernels: 73.4 us -> 61.1 us  [on_device(): pl.pallas_call(layer_body, out_shape=jax.ShapeDtypeStruct((HALF, D), bf16...]
    unnamed x2 -> x1, local copies, waits for them, and re-layouts: 3.72 us -> 1.77 us
    broadcast_in_dim x1 -> x0, local copies, waits for them, and re-layouts: 1.28 us -> none  [on_device(): norm_gain[None]]
where the time goes in v3:
time: 63 us; the launch traced here: 62.9 us
  Pallas kernels  61.1 us (97%)
  local copies, waits for them, and re-layouts  1.77 us (3%)
    pallas_call x1, Pallas kernels, on_device(): pl.pallas_call(layer_body, out_shape=jax.ShapeDtypeStruct((HALF, D), bf16...  61.1 us
    unnamed x1, local copies, waits for them, and re-layouts  1.77 us

profile of v3, /device:TPU:1, one launch (start us, length us, event | category | flops | bytes accessed | tf_op | source)
XLA Modules:
  0.0 62.9 jit_solution(6677301825334532001)
XLA Ops:
  0.0 61.1 %shard_map.163 = bf16[96,2048]{1,0:T(8,128)(2,1)} custom-call(bf16[192,1024]{1,0:T(8,128)(2,1)} %bitcast.7, bf16[8,128]{1,0:T(8,128)(2,1)} %bitcast.9, bf16[512,512]{1,0:T(8,128)(2,1)} %w_q_down.1, f32[1,512]{1,0:T(1,128)} %bitcast.10, bf16[512,1024]{1,0:T(8,128)(2,1)} %w_q_nope.1, bf16[512,512]{1,0:T(8,128)(2,1)} %w_q_rope.1, bf16[512,256]{1,0:T(8,128)(2,1)} %w_kv_down.1, ...), custom_call_target="tpu_custom_call" | custom-call | tf_op jit(solution)/shard_map/pallas_call | solution.py:667
  61.1 1.8 %copy.19 = bf16[1,96,2048]{2,1,0:T(8,128)(2,1)} copy(bf16[1,96,2048]{2,1,0:T(8,128)(2,1)} %bitcast.6) | data formatting | bytes 786432

commit v4 on v3

--- a/solution.py
+++ b/solution.py
@@ -331,7 +331,7 @@
     kv_pre = jnp.dot(hidden[mine, :], wkv[...], preferred_element_type=f32).astype(bf16)
     own0 = x * HALF
     own1 = SEQ // 2 + z * HALF
-    own_rows = pl.ds(pl.multiple_of(jnp.where(c == 0, own0, own1), HALF), HALF)
+    own_rows = pl.ds(pl.multiple_of(jnp.where(c == 1, own0, own1), HALF), HALF)
     kv[own_rows, :KR] = scaled_rows(kv_pre.astype(f32), kv_gain_s[...], KR).astype(bf16)
     kv[own_rows, KR:] = key_rope
 
@@ -357,12 +357,12 @@
         view = blk1(lax.rem(z + NZ - i, NZ))
         return remote(view, view, p1_ss.at[i], p1_rs.at[i], z_up)
 
-    @pl.when(c == 0)
+    @pl.when(c == 1)
     def _():
         for i in (1, 3, 2):
             first0(i).start()
 
-    @pl.when(c == 1)
+    @pl.when(c == 0)
     def _():
         for i in (1, 7, 2, 6, 3, 5, 4):
             first1(i).start()
@@ -420,12 +420,7 @@
             copy.start()
         sib(cls, n).start()
 
-    q_got("up2").wait_recv()
-    q_sib(0).start()
-    q_got("dn2").wait_recv()
-    q_sib(1).start()
-
-    @pl.when(c == 0)
+    @pl.when(c == 1)
     def _():
         for i in (1, 3, 2):
             first0_got(i).wait_recv()
@@ -433,6 +428,11 @@
             copy.start()
         sib(0, 0).start()
 
+
+    q_got("up2").wait_recv()
+    q_sib(0).start()
+    q_got("dn2").wait_recv()
+    q_sib(1).start()
 
     remote(halo.at[pl.ds(0, 16)], halo.at[pl.ds(0, 16)], halo_ss.at[0], halo_rs.at[0], next_dev).wait_recv()
     remote(halo.at[pl.ds(16, 16)], halo.at[pl.ds(16, 16)], halo_ss.at[1], halo_rs.at[1], next_dev).wait_recv()
@@ -467,6 +467,15 @@
     q_sib(2).start()
     for i in (8, 9, 10, 13):
         loads[i].wait()
+    @pl.when(c == 0)
+    def _():
+        for i in (1, 7, 2, 6, 3, 5, 4):
+            first1_got(i).wait_recv()
+        for copy in sends_after(1, 0):
+            copy.start()
+        sib(1, 0).start()
+        sib(1, 1).start()
+
     for i in range(3):
         q_sib_got(i).wait_recv()
     q_pre = jnp.dot(hidden[...], wq[...], preferred_element_type=f32).astype(bf16)
@@ -486,40 +495,35 @@
         )
         q_all[rows, :KR] = (absorbed * SCALE).astype(bf16)
 
-    @pl.when(c == 0)
+    @pl.when(c == 1)
     def _():
         acquire_own(0, 1)
         acquire_own(0, 2)
 
-    @pl.when(c == 1)
-    def _():
-        for i in (1, 7, 2, 6, 3, 5, 4):
-            first1_got(i).wait_recv()
-        for copy in sends_after(1, 0):
-            copy.start()
-        sib(1, 0).start()
-        sib(1, 1).start()
-
     steps = 2 * (SEQ // 2) // STEP
 
     def row_of(i):
-        cls = lax.rem(i + c, 2)
+        cls = lax.rem(i + 1 - c, 2)
         return pl.multiple_of(cls * (SEQ // 2) + (i // 2) * STEP, STEP)
 
     def acquire(i):
         for m in range(1, 4):
-            for cls in range(2):
-
-                @pl.when((i == 2 * m) & (c == cls))
-                def _():
-                    for n in (2 * m, 2 * m + 1):
-                        if n > 2 or cls == 1:
-                            acquire_own(cls, n)
+
+            @pl.when((i == 2 * m) & (c == 1))
+            def _():
+                for n in (2 * m + 1, 2 * m + 2):
+                    if n < 8:
+                        acquire_own(0, n)
+
+            @pl.when((i == 2 * m) & (c == 0))
+            def _():
+                for n in (2 * m, 2 * m + 1):
+                    acquire_own(1, n)
 
         @pl.when(lax.rem(i, 2) == 1)
         def _():
             for n in range(2):
-                at = (1 - c) * (SEQ // 2) + (i // 2) * STEP + n * UNIT
+                at = c * (SEQ // 2) + (i // 2) * STEP + n * UNIT
                 view = kv.at[pl.ds(at, UNIT)]
                 remote(view, view, sib_ss.at[i - 1 + n], sib_rs.at[i - 1 + n], other).wait_recv()
 
@@ -599,13 +603,16 @@
     def share(j):
         return remote(send_buf.at[j], recv_buf.at[j], out_ss.at[j], out_rs.at[j], other)
 
-    for j in range(4):
-        cols = slice(j * 512, (j + 1) * 512)
-        out_sum[:, cols] = out_sum[:, cols] + jnp.dot(att[...], woa[:, cols], preferred_element_type=f32)
-        send_buf[j] = out_sum[theirs, cols].astype(bf16)
+    def projected(rows, cols):
+        return out_sum[rows, cols] + jnp.dot(att[rows, :], woa[:, cols], preferred_element_type=f32)
+
+    blocks = [slice(j * 512, (j + 1) * 512) for j in range(4)]
+    for j, cols in enumerate(blocks):
+        send_buf[j] = projected(theirs, cols).astype(bf16)
         share(j).start()
-    for j in range(4):
-        cols = slice(j * 512, (j + 1) * 512)
+    for cols in blocks:
+        out_sum[mine, cols] = projected(mine, cols)
+    for j, cols in enumerate(blocks):
         share(j).wait_recv()
         out[:, cols] = (out_sum[mine, cols] + recv_buf[j].astype(f32)).astype(bf16)
 
@@ -620,8 +627,12 @@
     for j in range(4):
         share(j).wait_send()
 
-    @pl.when(c == 0)
-    def _():
+    @pl.when(c == 1)
+    def _():
+        for name in ("up1", "up2", "dn1", "dn2", "upf", "dnf"):
+            kv_send(name).wait_send()
+        for i in range(3):
+            kv_sib(i).wait_send()
         for i in range(1, NX):
             first0(i).wait_send()
         for n in range(8):
@@ -629,12 +640,8 @@
                 copy.wait_send()
             sib(0, n).wait_send()
 
-    @pl.when(c == 1)
-    def _():
-        for name in ("up1", "up2", "dn1", "dn2", "upf", "dnf"):
-            kv_send(name).wait_send()
-        for i in range(3):
-            kv_sib(i).wait_send()
+    @pl.when(c == 0)
+    def _():
         for i in range(1, NZ):
             first1(i).wait_send()
         for n in range(8):

time: 63 us -> 58.4 us (0.927)
  Pallas kernels: 61.1 us -> 56.5 us
    pallas_call x1, Pallas kernels: 61.1 us -> 56.5 us  [on_device(): pl.pallas_call(layer_body, out_shape=jax.ShapeDtypeStruct((HALF, D), bf16...]
where the time goes in v4:
time: 58.4 us; the launch traced here: 58.2 us
  Pallas kernels  56.5 us (97%)
  local copies, waits for them, and re-layouts  1.77 us (3%)
    pallas_call x1, Pallas kernels, on_device(): pl.pallas_call(layer_body, out_shape=jax.ShapeDtypeStruct((HALF, D), bf16...  56.5 us
    unnamed x1, local copies, waits for them, and re-layouts  1.77 us

profile of v4, /device:TPU:1, one launch (start us, length us, event | category | flops | bytes accessed | tf_op | source)
XLA Modules:
  0.0 58.2 jit_solution(4514828382692251216)
XLA Ops:
  0.0 56.5 %shard_map.163 = bf16[96,2048]{1,0:T(8,128)(2,1)} custom-call(bf16[192,1024]{1,0:T(8,128)(2,1)} %bitcast.7, bf16[8,128]{1,0:T(8,128)(2,1)} %bitcast.9, bf16[512,512]{1,0:T(8,128)(2,1)} %w_q_down.1, f32[1,512]{1,0:T(1,128)} %bitcast.10, bf16[512,1024]{1,0:T(8,128)(2,1)} %w_q_nope.1, bf16[512,512]{1,0:T(8,128)(2,1)} %w_q_rope.1, bf16[512,256]{1,0:T(8,128)(2,1)} %w_kv_down.1, ...), custom_call_target="tpu_custom_call" | custom-call | tf_op jit(solution)/shard_map/pallas_call | solution.py:674
  56.5 1.8 %copy.19 = bf16[1,96,2048]{2,1,0:T(8,128)(2,1)} copy(bf16[1,96,2048]{2,1,0:T(8,128)(2,1)} %bitcast.6) | data formatting | bytes 786432

commit v5 on v4

--- a/solution.py
+++ b/solution.py
@@ -30,7 +30,7 @@
 WIDE = 384
 UNIT = 384
 ROWS = HEADS * TOK
-MB = 384
+MB = 256
 STEP = 2 * UNIT
 SUB = 32
 SEQ = NZ * NX * TOK
@@ -108,6 +108,7 @@
     sin_s,
     kv,
     q_all,
+    q_sum,
     q_lat,
     q_nope,
     pool_in,
@@ -309,6 +310,7 @@
     halo_next.start()
     halo_prev.start()
 
+
     mine = pl.ds(c * HALF, HALF)
     loads[3].wait()
     key_pre = lax.dot_general(
@@ -353,6 +355,10 @@
         to = lax.rem(z + i, NZ)
         return remote(blk1(z), blk1(z), p1_ss.at[i], p1_rs.at[i], {"sp_0": to})
 
+    def first1_far():
+        view = blk1(lax.rem(z + 3, NZ))
+        return remote(view, view, p1_ss.at[4], p1_rs.at[4], z_down)
+
     def first1_got(i):
         view = blk1(lax.rem(z + NZ - i, NZ))
         return remote(view, view, p1_ss.at[i], p1_rs.at[i], z_up)
@@ -364,7 +370,7 @@
 
     @pl.when(c == 0)
     def _():
-        for i in (1, 7, 2, 6, 3, 5, 4):
+        for i in (1, 7, 2, 6, 5, 3):
             first1(i).start()
 
     q_got("up1").wait_recv()
@@ -462,6 +468,18 @@
         cols = slice(j * 512, (j + 1) * 512)
         out_sum[:, cols] = jnp.dot(pooled[...], wop[:, cols], preferred_element_type=f32)
 
+    @pl.when(c == 0)
+    def _():
+        first1_got(5).wait_recv()
+        first1_far().start()
+
+    def query_part(of):
+        at = pl.ds(pl.multiple_of(of * 512, 512), 512)
+        return jnp.dot(hidden[:, at], wq[at, :], preferred_element_type=f32)
+
+    q_sib_got(0).wait_recv()
+    q_sib_got(1).wait_recv()
+    q_sum[...] = query_part(y) + query_part(y1) + query_part(y2)
     q_got("upf").wait_recv()
     q_got("dnf").wait_recv()
     q_sib(2).start()
@@ -469,16 +487,15 @@
         loads[i].wait()
     @pl.when(c == 0)
     def _():
-        for i in (1, 7, 2, 6, 3, 5, 4):
+        for i in (1, 7, 2, 6, 3, 4):
             first1_got(i).wait_recv()
         for copy in sends_after(1, 0):
             copy.start()
         sib(1, 0).start()
         sib(1, 1).start()
 
-    for i in range(3):
-        q_sib_got(i).wait_recv()
-    q_pre = jnp.dot(hidden[...], wq[...], preferred_element_type=f32).astype(bf16)
+    q_sib_got(2).wait_recv()
+    q_pre = (q_sum[...] + query_part(y3)).astype(bf16)
     q_lat[...] = scaled_rows(q_pre.astype(f32), q_gain_s[...], QR).astype(bf16)
     q_nope[...] = jnp.dot(q_lat[...], wqn[...], preferred_element_type=f32).astype(bf16)
     q_rot = jnp.dot(q_lat[...], wqr[...], preferred_element_type=f32).astype(bf16).astype(f32)
@@ -498,7 +515,6 @@
     @pl.when(c == 1)
     def _():
         acquire_own(0, 1)
-        acquire_own(0, 2)
 
     steps = 2 * (SEQ // 2) // STEP
 
@@ -507,6 +523,10 @@
         return pl.multiple_of(cls * (SEQ // 2) + (i // 2) * STEP, STEP)
 
     def acquire(i):
+        @pl.when((i == 1) & (c == 1))
+        def _():
+            acquire_own(0, 2)
+
         for m in range(1, 4):
 
             @pl.when((i == 2 * m) & (c == 1))
@@ -642,8 +662,9 @@
 
     @pl.when(c == 0)
     def _():
-        for i in range(1, NZ):
+        for i in (1, 2, 3, 5, 6, 7):
             first1(i).wait_send()
+        first1_far().wait_send()
         for n in range(8):
             for copy in sends_after(1, n):
                 copy.wait_send()
@@ -699,6 +720,7 @@
             pltpu.VMEM((TOK, 128), f32),
             pltpu.VMEM((SEQ, WIDE), bf16),
             pltpu.VMEM((ROWS, WIDE), bf16),
+            pltpu.VMEM((TOK, QR), f32),
             pltpu.VMEM((TOK, QR), bf16),
             pltpu.VMEM((TOK, 1024), bf16),
             pltpu.VMEM((TOK, 512), bf16),

time: 58.4 us -> 58.5 us (level)
  no operation moved by 1% of the time
where the time goes in v5:
time: 58.5 us; the launch traced here: 58.3 us
  Pallas kernels  56.6 us (97%)
  local copies, waits for them, and re-layouts  1.77 us (3%)
    pallas_call x1, Pallas kernels, on_device(): pl.pallas_call(layer_body, out_shape=jax.ShapeDtypeStruct((HALF, D), bf16...  56.6 us
    unnamed x1, local copies, waits for them, and re-layouts  1.77 us

profile of v5, /device:TPU:1, one launch (start us, length us, event | category | flops | bytes accessed | tf_op | source)
XLA Modules:
  0.0 58.3 jit_solution(13424920467387627753)
XLA Ops:
  0.0 56.6 %shard_map.163 = bf16[96,2048]{1,0:T(8,128)(2,1)} custom-call(bf16[192,1024]{1,0:T(8,128)(2,1)} %bitcast.7, bf16[8,128]{1,0:T(8,128)(2,1)} %bitcast.9, bf16[512,512]{1,0:T(8,128)(2,1)} %w_q_down.1, f32[1,512]{1,0:T(1,128)} %bitcast.10, bf16[512,1024]{1,0:T(8,128)(2,1)} %w_q_nope.1, bf16[512,512]{1,0:T(8,128)(2,1)} %w_q_rope.1, bf16[512,256]{1,0:T(8,128)(2,1)} %w_kv_down.1, ...), custom_call_target="tpu_custom_call" | custom-call | tf_op jit(solution)/shard_map/pallas_call | solution.py:695
  56.6 1.8 %copy.19 = bf16[1,96,2048]{2,1,0:T(8,128)(2,1)} copy(bf16[1,96,2048]{2,1,0:T(8,128)(2,1)} %bitcast.6) | data formatting | bytes 786432

commit v6 on v5

--- a/solution.py
+++ b/solution.py
@@ -523,17 +523,13 @@
         return pl.multiple_of(cls * (SEQ // 2) + (i // 2) * STEP, STEP)
 
     def acquire(i):
-        @pl.when((i == 1) & (c == 1))
-        def _():
-            acquire_own(0, 2)
+        for n in range(2, 8):
+
+            @pl.when((i == n - 1) & (c == 1))
+            def _():
+                acquire_own(0, n)
 
         for m in range(1, 4):
-
-            @pl.when((i == 2 * m) & (c == 1))
-            def _():
-                for n in (2 * m + 1, 2 * m + 2):
-                    if n < 8:
-                        acquire_own(0, n)
 
             @pl.when((i == 2 * m) & (c == 0))
             def _():

time: 58.5 us -> 57.8 us (0.988)
  Pallas kernels: 56.6 us -> 55.9 us
    pallas_call x1, Pallas kernels: 56.6 us -> 55.9 us  [on_device(): pl.pallas_call(layer_body, out_shape=jax.ShapeDtypeStruct((HALF, D), bf16...]
where the time goes in v6:
time: 57.8 us; the launch traced here: 57.7 us
  Pallas kernels  55.9 us (97%)
  local copies, waits for them, and re-layouts  1.77 us (3%)
    pallas_call x1, Pallas kernels, on_device(): pl.pallas_call(layer_body, out_shape=jax.ShapeDtypeStruct((HALF, D), bf16...  55.9 us
    unnamed x1, local copies, waits for them, and re-layouts  1.77 us

profile of v6, /device:TPU:1, one launch (start us, length us, event | category | flops | bytes accessed | tf_op | source)
XLA Modules:
  0.0 57.7 jit_solution(4380114192811470480)
XLA Ops:
  0.0 55.9 %shard_map.163 = bf16[96,2048]{1,0:T(8,128)(2,1)} custom-call(bf16[192,1024]{1,0:T(8,128)(2,1)} %bitcast.7, bf16[8,128]{1,0:T(8,128)(2,1)} %bitcast.9, bf16[512,512]{1,0:T(8,128)(2,1)} %w_q_down.1, f32[1,512]{1,0:T(1,128)} %bitcast.10, bf16[512,1024]{1,0:T(8,128)(2,1)} %w_q_nope.1, bf16[512,512]{1,0:T(8,128)(2,1)} %w_q_rope.1, bf16[512,256]{1,0:T(8,128)(2,1)} %w_kv_down.1, ...), custom_call_target="tpu_custom_call" | custom-call | tf_op jit(solution)/shard_map/pallas_call | solution.py:691
  55.9 1.8 %copy.19 = bf16[1,96,2048]{2,1,0:T(8,128)(2,1)} copy(bf16[1,96,2048]{2,1,0:T(8,128)(2,1)} %bitcast.6) | data formatting | bytes 786432
